TPU v7x, 128 devices: a whole 4x4x4 slice. The times are simulated.
128 devices in a mesh: sp: 16 (over z, y), dp: 8 (over x, core).
Axes of the slice: x: 4, y: 4, z: 4, core: 2. Of those that a mesh axis runs over, the one named last changes fastest.
Arguments:
- tokens: bfloat16 [8, 4096, 2048], P('dp', 'sp'), may hold values from -6 to 6
- w_query: bfloat16 [2048, 2048], P('dp', 'sp'), may hold values from -0.125 to 0.125
- w_key: bfloat16 [2048, 1024], P('dp', 'sp'), may hold values from -0.125 to 0.125
- w_value: bfloat16 [2048, 1024], P('dp', 'sp'), may hold values from -0.125 to 0.125
- w_out: bfloat16 [2048, 2048], P('dp', 'sp'), may hold values from -0.25 to 0.25
- qk_gain: float32 [2, 128], replicated, may hold values from 0.9 to 24
Outputs:
- mixed_out: bfloat16 [8, 4096, 2048], P('dp', 'sp')
All inputs are finite; a program needn't handle non-finite values.
Results may differ from a plain program's by a relative error of at most 0.006.
The roundings to bfloat16 on the way count: a program that leaves them out, or rounds other values in their place, can miss the bound.
Values may be sent and summed in bfloat16 or wider, within the bound.
A program may use at most 64 MiB of HBM per device.

v0:
```python
import math

import jax
import jax.numpy as jnp
import numpy as np
from jax import lax
from jax.sharding import PartitionSpec as P

HQ = 16
KV = 8
HD = 128
GRID_W = 64


ROPE_BASE = 10000.0
EPS = 1e-06


def in_order(blocks, dim):
    blocks = jnp.moveaxis(blocks, 0, dim)
    shape = blocks.shape
    return blocks.reshape(*shape[:dim], shape[dim] * shape[dim + 1], *shape[dim + 2 :])


def sent_to_all(x, axis):
    copies = jnp.broadcast_to(x, (lax.axis_size(axis), *x.shape))
    return lax.all_to_all(copies, axis, split_axis=0, concat_axis=0, tiled=True)


def collect(x, axis, dim):
    return in_order(sent_to_all(x, axis), dim)


def angles(positions):
    quarter = jnp.arange(0, HD // 2, 2, dtype=jnp.float32)
    inv_freq = ROPE_BASE ** (-quarter / (HD // 2))
    row_pos = (positions // GRID_W).astype(jnp.float32)
    col_pos = (positions % GRID_W).astype(jnp.float32)
    angle_table = jnp.concatenate(
        [row_pos[:, None] * inv_freq, col_pos[:, None] * inv_freq], axis=1
    )
    return (jnp.cos(angle_table), jnp.sin(angle_table))


def prepare(raw_proj, gain_row, cosine, sine_table):
    normed = (
        raw_proj * lax.rsqrt(jnp.mean(raw_proj * raw_proj, axis=-1, keepdims=True) + EPS) * gain_row
    )
    pair_view = normed.reshape(raw_proj.shape[:-1] + (HD // 2, 2))
    first_half = pair_view[..., 0]
    second = pair_view[..., 1]
    cos_b = cosine[:, None, :]
    sin_b = sine_table[:, None, :]
    turned = jnp.stack(
        [first_half * cos_b - second * sin_b, first_half * sin_b + second * cos_b], axis=-1
    )
    return turned.reshape(raw_proj.shape).astype(jnp.bfloat16)


def attend_head(query_rows, key_rows, value_rows):
    seq_len = query_rows.shape[0]
    block_len = math.gcd(seq_len, 512)
    blocks = query_rows.reshape(seq_len // block_len, block_len, HD)

    def one_block(row_block):
        scores = jnp.dot(row_block, key_rows.T, preferred_element_type=jnp.float32) * HD ** (-0.5)
        top_score = jnp.max(scores, axis=1, keepdims=True)
        weights = jnp.exp(scores - top_score)
        row_total = jnp.sum(weights, axis=1, keepdims=True)
        probs_bf = (weights / row_total).astype(jnp.bfloat16)
        return jnp.dot(probs_bf, value_rows, preferred_element_type=jnp.float32).astype(
            jnp.bfloat16
        )

    return lax.map(one_block, blocks).reshape(seq_len, HD)


def project(own_rows, weight):
    col_full = collect(weight, "sp", 1)
    return jnp.dot(
        own_rows,
        lax.all_gather(col_full, "dp", axis=0, tiled=True),
        preferred_element_type=jnp.float32,
    )


def on_device(tokens, w_query, w_key, w_value, w_out, qk_gain):
    own_rows = tokens[0]
    n_seqdev = lax.axis_size("sp")
    tok_local = own_rows.shape[0]
    positions = lax.axis_index("sp") * tok_local + jnp.arange(tok_local, dtype=jnp.int32)
    cosine, sine_table = angles(positions)
    heads_dev = HQ // n_seqdev
    group_size = HQ // KV
    kv_dev = max(1, heads_dev // group_size)
    chosen = (np.arange(n_seqdev) * heads_dev // group_size)[:, None] + np.arange(kv_dev)[None, :]
    chosen = chosen.reshape(-1)
    key_all = prepare(
        project(own_rows, w_key).reshape(tok_local, KV, HD), qk_gain[1], cosine, sine_table
    )
    values = project(own_rows, w_value).astype(jnp.bfloat16).reshape(tok_local, KV, HD)
    key_send = key_all[:, chosen, :].reshape(tok_local, -1)
    value_send = values[:, chosen, :].reshape(tok_local, -1)
    raw_proj = project(own_rows, w_query).reshape(tok_local, HQ, HD)
    query_heads = lax.all_to_all(
        prepare(raw_proj, qk_gain[0], cosine, sine_table).reshape(tok_local, HQ * HD),
        "sp",
        split_axis=1,
        concat_axis=0,
        tiled=True,
    )
    key_heads = lax.all_to_all(key_send, "sp", split_axis=1, concat_axis=0, tiled=True)
    value_heads = lax.all_to_all(value_send, "sp", split_axis=1, concat_axis=0, tiled=True)
    outputs = attend_head(query_heads, key_heads[:, 0:HD], value_heads[:, 0:HD])
    token_rows = lax.all_to_all(outputs, "sp", split_axis=0, concat_axis=1, tiled=True)
    return project(token_rows, w_out).astype(jnp.bfloat16)[None]


def solution(mesh):
    in_specs = (
        P("dp", "sp", None),
        P("dp", "sp"),
        P("dp", "sp"),
        P("dp", "sp"),
        P("dp", "sp"),
        P(),
    )
    out_specs = P("dp", "sp", None)
    return jax.shard_map(
        on_device, mesh=mesh, in_specs=in_specs, out_specs=out_specs, check_vma=False
    )
```

profile of v0, /device:TPU:1, one launch (start us, length us, event | category | flops | bytes accessed | tf_op | source)
XLA Modules:
  0.0 288.5 jit_solution(16202396729736009710)
XLA Ops:
  7.5 18.9 %all_to_all.84 = bf16[16,256,64]{1,2,0:T(8,128)(2,1)} all-to-all(bf16[16,256,64]{1,2,0:T(8,128)(2,1)S(1)} %broadcast_in_dim.42), channel_id=1, replica_groups=mesh['sp'=16,'dp'=8] {'sp'}, dimensions={0} | all-to-all | bytes 1048576 | tf_op jit(solution)/shard_map/all_to_all | solution.py:27
  27.3 13.2 %all_to_all.85 = bf16[16,256,64]{1,2,0:T(8,128)(2,1)} all-to-all(bf16[16,256,64]{1,2,0:T(8,128)(2,1)S(1)} %broadcast_in_dim.44), channel_id=1, replica_groups=mesh['sp'=16,'dp'=8] {'sp'}, dimensions={0} | all-to-all | bytes 1048576 | tf_op jit(solution)/shard_map/all_to_all | solution.py:27
  41.6 17.9 %all_to_all.86 = bf16[16,256,128]{1,2,0:T(8,128)(2,1)} all-to-all(bf16[16,256,128]{1,2,0:T(8,128)(2,1)S(1)} %broadcast_in_dim.23), channel_id=1, replica_groups=mesh['sp'=16,'dp'=8] {'sp'}, dimensions={0} | all-to-all | bytes 2097152 | tf_op jit(solution)/shard_map/all_to_all | solution.py:27
  60.8 3.7 %all-to-all-start.7 = ((bf16[16,256,128]{1,2,0:T(8,128)(2,1)}), bf16[16,256,128]{1,2,0:T(8,128)(2,1)S(1)}, u32[]{:S(2)}, u32[]{:S(2)}) async-start(bf16[16,256,128]{1,2,0:T(8,128)(2,1)} %broadcast_in_dim.46), calls=%async_computation.7 | async-start | bytes 2097152 | tf_op jit(solution)/shard_map/all_to_all | solution.py:27
  64.9 3.5 %multiply_reduce_fusion.2 = (f32[256,8]{0,1:T(8,128)S(1)}, f32[256,8,128]{0,2,1:T(8,128)S(1)}) fusion(bf16[8,128,2048]{2,1,0:T(8,128)(2,1)} %bitcast.98, bf16[1,256,2048]{2,1,0:T(8,128)(2,1)S(1)} %copy-done), kind=kOutput, calls=%fused_computation.28 | convolution fusion | flops 1074264064 | bytes 6299648 | tf_op jit(solution)/shard_map/dot_general | solution.py:80
  69.8 1.6 gather_fusion
  71.5 6.7 %all-to-all-done.7 = bf16[16,256,128]{1,2,0:T(8,128)(2,1)S(1)} async-done(((bf16[16,256,128]{1,2,0:T(8,128)(2,1)}), bf16[16,256,128]{1,2,0:T(8,128)(2,1)S(1)}, u32[]{:S(2)}, u32[]{:S(2)}) %all-to-all-start.7) | async-done | bytes 1048608 | tf_op jit(solution)/shard_map/all_to_all | solution.py:27
  79.2 3.8 %all-to-all-start.3 = ((bf16[256,16,128]{2,0,1:T(8,128)(2,1)}), bf16[256,16,128]{2,0,1:T(8,128)(2,1)S(1)}, u32[]{:S(2)}, u32[]{:S(2)}) async-start(bf16[256,16,128]{2,0,1:T(8,128)(2,1)} %bitcast.17), calls=%async_computation.3 | async-start | bytes 2097152 | tf_op jit(solution)/shard_map/all_to_all | solution.py:112
  83.0 16.5 %all-gather.9.cloned.1.call-done = bf16[2048,1024]{0,1:T(8,128)(2,1)} async-done(((bf16[256,1024]{0,1:T(8,128)(2,1)}), bf16[2048,1024]{0,1:T(8,128)(2,1)}) %all-gather.9.cloned.1.call-update) | async-done | bytes 4194320 | tf_op jit(solution)/shard_map/all_gather | solution.py:82
  99.5 3.5 %fusion.11 = bf16[32,8,8,128]{3,2,1,0:T(8,128)(2,1)S(1)} fusion(bf16[2048,1024]{0,1:T(8,128)(2,1)} %all-gather.9.cloned.1.call-done, bf16[1,256,2048]{2,1,0:T(8,128)(2,1)S(1)} %copy-done), kind=kOutput, calls=%fused_computation.20 | convolution fusion | flops 1074003968 | bytes 5767168 | tf_op jit(solution)/shard_map/dot_general | solution.py:80
  103.1 1.7 gather_fusion.1
  104.7 50.8 %all-gather.5.cloned.1.call-done = bf16[2048,2048]{0,1:T(8,128)(2,1)} async-done(((bf16[256,2048]{0,1:T(8,128)(2,1)}), bf16[2048,2048]{0,1:T(8,128)(2,1)}) %all-gather.5.cloned.1.call-update) | async-done | bytes 8388624 | tf_op jit(solution)/shard_map/all_gather | solution.py:82
  155.5 7.2 %multiply_reduce_fusion.1 = (f32[256,16]{0,1:T(8,128)S(1)}, f32[256,16,128]{0,2,1:T(8,128)}) fusion(bf16[16,128,2048]{2,1,0:T(8,128)(2,1)} %bitcast.97, bf16[1,256,2048]{2,1,0:T(8,128)(2,1)S(1)} %copy-done), kind=kOutput, calls=%fused_computation.18 | convolution fusion | flops 2148528128 | bytes 11550720 | tf_op jit(solution)/shard_map/dot_general | solution.py:80
  162.8 6.8 %all-to-all-start.5 = ((bf16[256,16,128]{2,0,1:T(8,128)(2,1)}), bf16[256,16,128]{2,0,1:T(8,128)(2,1)}, u32[]{:S(2)}, u32[]{:S(2)}) async-start(bf16[256,16,128]{2,0,1:T(8,128)(2,1)} %bitcast.22), calls=%async_computation.5 | async-start | bytes 2097152 | tf_op jit(solution)/shard_map/all_to_all | solution.py:113
  169.5 3.3 %multiply_multiply_fusion = f32[256,16,128]{0,2,1:T(8,128)} fusion(f32[256,16,128]{0,2,1:T(8,128)} %get-tuple-element.56, f32[128]{0:T(128)S(1)} %get-tuple-element.52, f32[256,16]{0,1:T(8,128)S(1)} %add_rsqrt_fusion), kind=kLoop, calls=%fused_computation.17 | loop fusion | flops 1048576 | bytes 4211200 | tf_op jit(solution)/shard_map/mul | solution.py:47
  172.8 3.4 %reshape.170 = f32[256,16,64,2]{0,3,2,1:T(2,128)} reshape(f32[256,16,128]{0,2,1:T(8,128)} %multiply_multiply_fusion) | data formatting | bytes 4194304 | tf_op jit(solution)/shard_map/reshape | solution.py:49
  176.3 4.3 %subtract_convert_fusion = (bf16[256,16,64,1]{0,3,2,1:T(2,128)(2,1)S(1)}, bf16[256,16,64,1]{0,3,2,1:T(2,128)(2,1)S(1)}) fusion(f32[256,16,64,2]{0,3,2,1:T(2,128)} %reshape.170, f32[256,64]{0,1:T(8,128)S(1)} %get-tuple-element.50, f32[256,64]{0,1:T(8,128)S(1)} %get-tuple-element.49), kind=kLoop, calls=%fused_computation.30 | loop fusion | flops 2097152 | bytes 3276800 | tf_op jit(solution)/shard_map/convert.2
  180.6 2.4 pad_maximum_fusion
  183.5 1.3 copy.20
  186.1 5.3 %all-to-all-start.1 = ((bf16[256,16,128]{2,0,1:T(8,128)(2,1)}), bf16[256,16,128]{2,0,1:T(8,128)(2,1)S(1)}, u32[]{:S(2)}, u32[]{:S(2)}) async-start(bf16[256,16,128]{2,0,1:T(8,128)(2,1)} %copy.20), calls=%async_computation.1 | async-start | bytes 2097152 | tf_op jit(solution)/shard_map/all_to_all | solution.py:105
  192.0 15.3 %all-to-all-done.1 = bf16[256,16,128]{2,0,1:T(8,128)(2,1)S(1)} async-done(((bf16[256,16,128]{2,0,1:T(8,128)(2,1)}), bf16[256,16,128]{2,0,1:T(8,128)(2,1)S(1)}, u32[]{:S(2)}, u32[]{:S(2)}) %all-to-all-start.1) | async-done | bytes 1048608 | tf_op jit(solution)/shard_map/all_to_all | solution.py:105
  207.3 47.5 %while.10 = (s32[]{:T(128)}, bf16[8,512,128]{2,1,0:T(8,128)(2,1)S(1)}, bf16[8,512,128]{2,1,0:T(8,128)(2,1)S(1)}, bf16[4096,128]{1,0:T(8,128)(2,1)S(1)}, bf16[4096,128]{1,0:T(8,128)(2,1)}, /*index=5*/s32[]{:T(128)}) while((s32[]{:T(128)}, bf16[8,512,128]{2,1,0:T(8,128)(2,1)S(1)}, bf16[8,512,128]{2,1,0:T(8,128)(2,1)S(1)}, ...), condition=%wide.region_5.6_spmd, body=%wide.region_2.5_spmd.sunk | while | flops 1092680704 | bytes 27535436 | solution.py:75
  207.3 1.3 multiply_reduce_fusion.4
  208.6 1.5 fusion.35
  210.1 3.1 %fusion.36 = bf16[8,512,128]{2,1,0:T(8,128)(2,1)S(1)} fusion(bf16[8,512,128]{2,1,0:T(8,128)(2,1)S(1)} %get-tuple-element.103, s32[]{:T(128)} %get-tuple-element.102, bf16[4096,128]{1,0:T(8,128)(2,1)} %get-tuple-element.112, f32[512,4096]{1,0:T(8,128)S(1)} %get-tuple-element.94, f32[512]{0:T(512)S(1)} %fusion.35, f32[512]{0:T(512)S(1)} %get-tuple-element.95), kind=kOutput, calls=%fused_computation.9.clone.1 | convolution fusion | flops 545325056 | bytes 9572356 | tf_op jit(solution)/shard_map/while/body/eval_jaxpr/dot_general | solution.py:71
  213.2 1.3 multiply_reduce_fusion.4
  214.6 1.5 fusion.35
  216.1 3.1 %fusion.36 = bf16[8,512,128]{2,1,0:T(8,128)(2,1)S(1)} fusion(bf16[8,512,128]{2,1,0:T(8,128)(2,1)S(1)} %get-tuple-element.103, s32[]{:T(128)} %get-tuple-element.102, bf16[4096,128]{1,0:T(8,128)(2,1)} %get-tuple-element.112, f32[512,4096]{1,0:T(8,128)S(1)} %get-tuple-element.94, f32[512]{0:T(512)S(1)} %fusion.35, f32[512]{0:T(512)S(1)} %get-tuple-element.95), kind=kOutput, calls=%fused_computation.9.clone.1 | convolution fusion | flops 545325056 | bytes 9572356 | tf_op jit(solution)/shard_map/while/body/eval_jaxpr/dot_general | solution.py:71
  219.1 1.3 multiply_reduce_fusion.4
  220.5 1.5 fusion.35
  222.0 3.1 %fusion.36 = bf16[8,512,128]{2,1,0:T(8,128)(2,1)S(1)} fusion(bf16[8,512,128]{2,1,0:T(8,128)(2,1)S(1)} %get-tuple-element.103, s32[]{:T(128)} %get-tuple-element.102, bf16[4096,128]{1,0:T(8,128)(2,1)} %get-tuple-element.112, f32[512,4096]{1,0:T(8,128)S(1)} %get-tuple-element.94, f32[512]{0:T(512)S(1)} %fusion.35, f32[512]{0:T(512)S(1)} %get-tuple-element.95), kind=kOutput, calls=%fused_computation.9.clone.1 | convolution fusion | flops 545325056 | bytes 9572356 | tf_op jit(solution)/shard_map/while/body/eval_jaxpr/dot_general | solution.py:71
  225.1 1.3 multiply_reduce_fusion.4
  226.4 1.5 fusion.35
  227.9 3.1 %fusion.36 = bf16[8,512,128]{2,1,0:T(8,128)(2,1)S(1)} fusion(bf16[8,512,128]{2,1,0:T(8,128)(2,1)S(1)} %get-tuple-element.103, s32[]{:T(128)} %get-tuple-element.102, bf16[4096,128]{1,0:T(8,128)(2,1)} %get-tuple-element.112, f32[512,4096]{1,0:T(8,128)S(1)} %get-tuple-element.94, f32[512]{0:T(512)S(1)} %fusion.35, f32[512]{0:T(512)S(1)} %get-tuple-element.95), kind=kOutput, calls=%fused_computation.9.clone.1 | convolution fusion | flops 545325056 | bytes 9572356 | tf_op jit(solution)/shard_map/while/body/eval_jaxpr/dot_general | solution.py:71
  231.0 1.3 multiply_reduce_fusion.4
  232.3 1.5 fusion.35
  233.8 3.2 %fusion.36 = bf16[8,512,128]{2,1,0:T(8,128)(2,1)S(1)} fusion(bf16[8,512,128]{2,1,0:T(8,128)(2,1)S(1)} %get-tuple-element.103, s32[]{:T(128)} %get-tuple-element.102, bf16[4096,128]{1,0:T(8,128)(2,1)} %get-tuple-element.112, f32[512,4096]{1,0:T(8,128)S(1)} %get-tuple-element.94, f32[512]{0:T(512)S(1)} %fusion.35, f32[512]{0:T(512)S(1)} %get-tuple-element.95), kind=kOutput, calls=%fused_computation.9.clone.1 | convolution fusion | flops 545325056 | bytes 9572356 | tf_op jit(solution)/shard_map/while/body/eval_jaxpr/dot_general | solution.py:71
  237.0 1.3 multiply_reduce_fusion.4
  238.3 1.5 fusion.35
  239.8 3.1 %fusion.36 = bf16[8,512,128]{2,1,0:T(8,128)(2,1)S(1)} fusion(bf16[8,512,128]{2,1,0:T(8,128)(2,1)S(1)} %get-tuple-element.103, s32[]{:T(128)} %get-tuple-element.102, bf16[4096,128]{1,0:T(8,128)(2,1)} %get-tuple-element.112, f32[512,4096]{1,0:T(8,128)S(1)} %get-tuple-element.94, f32[512]{0:T(512)S(1)} %fusion.35, f32[512]{0:T(512)S(1)} %get-tuple-element.95), kind=kOutput, calls=%fused_computation.9.clone.1 | convolution fusion | flops 545325056 | bytes 9572356 | tf_op jit(solution)/shard_map/while/body/eval_jaxpr/dot_general | solution.py:71
  242.9 1.3 multiply_reduce_fusion.4
  244.2 1.5 fusion.35
  245.8 3.1 %fusion.36 = bf16[8,512,128]{2,1,0:T(8,128)(2,1)S(1)} fusion(bf16[8,512,128]{2,1,0:T(8,128)(2,1)S(1)} %get-tuple-element.103, s32[]{:T(128)} %get-tuple-element.102, bf16[4096,128]{1,0:T(8,128)(2,1)} %get-tuple-element.112, f32[512,4096]{1,0:T(8,128)S(1)} %get-tuple-element.94, f32[512]{0:T(512)S(1)} %fusion.35, f32[512]{0:T(512)S(1)} %get-tuple-element.95), kind=kOutput, calls=%fused_computation.9.clone.1 | convolution fusion | flops 545325056 | bytes 9572356 | tf_op jit(solution)/shard_map/while/body/eval_jaxpr/dot_general | solution.py:71
  248.9 1.3 multiply_reduce_fusion.4
  250.2 1.5 fusion.35
  251.8 3.1 %fusion.36 = bf16[8,512,128]{2,1,0:T(8,128)(2,1)S(1)} fusion(bf16[8,512,128]{2,1,0:T(8,128)(2,1)S(1)} %get-tuple-element.103, s32[]{:T(128)} %get-tuple-element.102, bf16[4096,128]{1,0:T(8,128)(2,1)} %get-tuple-element.112, f32[512,4096]{1,0:T(8,128)S(1)} %get-tuple-element.94, f32[512]{0:T(512)S(1)} %fusion.35, f32[512]{0:T(512)S(1)} %get-tuple-element.95), kind=kOutput, calls=%fused_computation.9.clone.1 | convolution fusion | flops 545325056 | bytes 9572356 | tf_op jit(solution)/shard_map/while/body/eval_jaxpr/dot_general | solution.py:71
  254.8 19.8 %all_to_all.87 = bf16[16,256,128]{2,1,0:T(8,128)(2,1)S(1)} all-to-all(bf16[16,256,128]{2,1,0:T(8,128)(2,1)S(1)} %bitcast.95), channel_id=1, replica_groups=mesh['sp'=16,'dp'=8] {'sp'}, dimensions={0} | all-to-all | bytes 2097152 | tf_op jit(solution)/shard_map/all_to_all | solution.py:115
  275.2 6.7 %fusion.10 = bf16[1,256,2048]{2,1,0:T(8,128)(2,1)} fusion(bf16[256,2048]{0,1:T(8,128)(2,1)S(1)} %bitcast.96, bf16[2048,2048]{0,1:T(8,128)(2,1)} %all-gather.11.cloned.1.call-done), kind=kOutput, calls=%fused_computation.16 | convolution fusion | flops 2148007936 | bytes 10485760 | tf_op jit(solution)/shard_map/dot_general | solution.py:80
  (47 shorter events, 9.9 us)
Async XLA Ops:
  6.5 58.3 %copy-start = (bf16[1,256,2048]{2,1,0:T(8,128)(2,1)S(1)}, bf16[1,256,2048]{2,1,0:T(8,128)(2,1)}, u32[]{:S(2)}) copy-start(bf16[1,256,2048]{2,1,0:T(8,128)(2,1)} %param.11) | copy-start | bytes 3145732
  6.5 57.9 %copy-start.5 = (s32[16]{0:T(128)S(1)}, s32[16]{0:T(128)}, u32[]{:S(2)}) copy-start(s32[16]{0:T(128)} %constant.81) | copy-start | bytes 196
  6.5 53.0 %copy-start.3 = (bf16[256,128]{1,0:T(8,128)(2,1)S(1)}, bf16[256,128]{1,0:T(8,128)(2,1)}, u32[]{:S(2)}) copy-start(bf16[256,128]{1,0:T(8,128)(2,1)} %param.15) | copy-start | bytes 196612
  6.5 58.3 %copy-start.4 = (f32[2,128]{1,0:T(2,128)S(1)}, f32[2,128]{1,0:T(2,128)}, u32[]{:S(2)}) copy-start(f32[2,128]{1,0:T(2,128)} %param.16) | copy-start | bytes 3076
  6.5 58.3 %all-gather.7.cloned.1.call-start = ((), (), s32[]{:S(2)}) async-start(), calls=%async_computation.9 | async-start | bytes 4718592 | tf_op jit(solution)/shard_map/all_gather | solution.py:82
  26.4 73.1 %all-gather.9.cloned.1.call-start = ((), (), s32[]{:S(2)}) async-start(), calls=%async_computation.10 | async-start | bytes 4718592 | tf_op jit(solution)/shard_map/all_gather | solution.py:82
  40.5 115.0 %all-gather.5.cloned.1.call-start = ((), (), s32[]{:S(2)}) async-start(), calls=%async_computation.8 | async-start | bytes 9437184 | tf_op jit(solution)/shard_map/all_gather | solution.py:82
  60.8 17.4 %all-to-all-start.7 = ((bf16[16,256,128]{1,2,0:T(8,128)(2,1)}), bf16[16,256,128]{1,2,0:T(8,128)(2,1)S(1)}, u32[]{:S(2)}, u32[]{:S(2)}) async-start(bf16[16,256,128]{1,2,0:T(8,128)(2,1)} %broadcast_in_dim.46), calls=%async_computation.7 | async-start | bytes 2097152 | tf_op jit(solution)/shard_map/all_to_all | solution.py:27
  78.2 1.0 copy-start.2
  79.2 83.5 %all-to-all-start.3 = ((bf16[256,16,128]{2,0,1:T(8,128)(2,1)}), bf16[256,16,128]{2,0,1:T(8,128)(2,1)S(1)}, u32[]{:S(2)}, u32[]{:S(2)}) async-start(bf16[256,16,128]{2,0,1:T(8,128)(2,1)} %bitcast.17), calls=%async_computation.3 | async-start | bytes 2097152 | tf_op jit(solution)/shard_map/all_to_all | solution.py:112
  162.8 23.3 %all-to-all-start.5 = ((bf16[256,16,128]{2,0,1:T(8,128)(2,1)}), bf16[256,16,128]{2,0,1:T(8,128)(2,1)}, u32[]{:S(2)}, u32[]{:S(2)}) async-start(bf16[256,16,128]{2,0,1:T(8,128)(2,1)} %bitcast.22), calls=%async_computation.5 | async-start | bytes 2097152 | tf_op jit(solution)/shard_map/all_to_all | solution.py:113
  186.1 21.2 %all-to-all-start.1 = ((bf16[256,16,128]{2,0,1:T(8,128)(2,1)}), bf16[256,16,128]{2,0,1:T(8,128)(2,1)S(1)}, u32[]{:S(2)}, u32[]{:S(2)}) async-start(bf16[256,16,128]{2,0,1:T(8,128)(2,1)} %copy.20), calls=%async_computation.1 | async-start | bytes 2097152 | tf_op jit(solution)/shard_map/all_to_all | solution.py:105
  191.4 83.8 %all-gather.11.cloned.1.call-start = ((), (), s32[]{:S(2)}) async-start(), calls=%async_computation.11 | async-start | bytes 9437184 | tf_op jit(solution)/shard_map/all_gather | solution.py:82
  274.7 7.3 %copy-start.1 = (bf16[1,256,2048]{2,1,0:T(8,128)(2,1)S(1)}, bf16[1,256,2048]{2,1,0:T(8,128)(2,1)}, u32[]{:S(2)}) copy-start(bf16[1,256,2048]{2,1,0:T(8,128)(2,1)} %param.11) | copy-start | bytes 3145732
Sparse Core Ops, SparseCore 0:
  26.5 34.7 all-gather.6
  63.0 36.4 all-gather.8
  101.2 54.3 all-gather.4
  193.6 55.4 all-gather.10
where the time goes:
time: 290 us; the launch traced here: 289 us
  waiting for transfers between devices  91.1 us (31%)
  blocking collectives  69.9 us (24%)
  matrix products  56.2 us (19%)
  other arithmetic  22.9 us (8%)
  starting transfers between devices  19.7 us (7%)
  local copies, waits for them, and re-layouts  15.2 us (5%)
  between operations  13.4 us (5%)
    all_gather x4, waiting for transfers between devices, project(): lax.all_gather(col_full, 'dp', axis=0, tiled=True)  67.3 us
    all_to_all x3, blocking collectives, sent_to_all(): return lax.all_to_all(copies, axis, split_axis=0, concat_axis=0, tiled=True)  50 us
    dot_general x8, matrix products, one_block(): jnp.dot(probs_bf, value_rows, preferred_element_type=jnp.float32)  24.7 us
    dot_general x4, matrix products, project(): jnp.dot(own_rows, lax.all_gather(col_full, 'dp', axis=0, tiled=True), pre...  20.9 us
    all_to_all x1, blocking collectives, on_device(): lax.all_to_all(outputs, 'sp', split_axis=0, concat_axis=1, tiled=True)  19.8 us
    all_to_all x1, waiting for transfers between devices, on_device(): lax.all_to_all(prepare(raw_proj, qk_gain[0], cosine, sine_table).reshape(...  15.3 us
    reduce_sum x8, other arithmetic, one_block(): row_total = jnp.sum(weights, axis=1, keepdims=True)  12.1 us
    dot_general x8, matrix products, one_block(): jnp.dot(row_block, key_rows.T, preferred_element_type=jnp.float32)  10.7 us
  transfers between devices with their start and end apart: 8, of which 5 were waited for; matrix products, arithmetic and copies ran while one was open for 30% of the time, Pallas kernels for 0%

commit v1 on v0

v1 whole, which is shorter than its diff:
```python
import functools
import math

import jax
import jax.numpy as jnp
import numpy as np
from jax import lax
from jax.experimental import pallas as pl
from jax.experimental.pallas import tpu as pltpu
from jax.sharding import PartitionSpec as P

HQ = 16
KV = 8
HD = 128
GRID_W = 64
ROPE_BASE = 10000.0
EPS = 1e-06
ROWS = 256
BF = jnp.bfloat16
F32 = jnp.float32


def rope_tables():
    quarter = np.arange(0, HD // 2, 2, dtype=np.float32)
    inv_freq = np.float32(ROPE_BASE) ** (-quarter / np.float32(HD // 2))
    angle = np.arange(GRID_W, dtype=np.float32)[:, None] * inv_freq.astype(np.float32)
    angle = np.repeat(angle, 2, axis=1).astype(np.float64)
    angle = np.concatenate([angle, angle], axis=1)
    return np.cos(angle).astype(np.float32), np.sin(angle).astype(np.float32)


def kernel(
    tok_hbm, wqkv_hbm, wo_hbm, gain_ref, cos_ref, sin_ref,
    out_ref,
    X, W, WO, QT, KVB, S, ACC, AO, ATT,
    loc, tok_s, tok_r, wy_s, wy_r, wx_s, wx_r, wp_s, wp_r,
    oz_s, oz_r, oy_s, oy_r, ox_s, ox_r, op_s, op_r,
    kv_s, kv_r, at_s, at_r,
):
    sp = lax.axis_index("sp")
    dp = lax.axis_index("dp")
    z, y = sp // 4, sp % 4
    x, c = dp // 2, dp % 2

    def ring(v, d):
        return (v + d + 4) % 4

    def to(src, dst, ss, rs, dz=0, dy=0, dx=0, other=False):
        return pltpu.make_async_remote_copy(
            src_ref=src, dst_ref=dst, send_sem=ss, recv_sem=rs,
            device_id={
                "sp": ring(z, dz) * 4 + ring(y, dy),
                "dp": ring(x, dx) * 2 + ((1 - c) if other else c),
            },
            device_id_type=pl.DeviceIdType.MESH,
        )

    barrier = pltpu.get_barrier_semaphore()
    for kw in (
        dict(dz=1), dict(dz=-1), dict(dz=2), dict(dy=1), dict(dy=-1), dict(dy=2),
        dict(dx=1), dict(dx=-1), dict(other=True),
    ):
        pl.semaphore_signal(
            barrier, inc=1,
            device_id={
                "sp": ring(z, kw.get("dz", 0)) * 4 + ring(y, kw.get("dy", 0)),
                "dp": ring(x, kw.get("dx", 0)) * 2 + ((1 - c) if kw.get("other") else c),
            },
            device_id_type=pl.DeviceIdType.MESH,
        )
    pl.semaphore_wait(barrier, 9)

    lo, hi = pl.ds(0, 128), pl.ds(128, 128)

    def tok(i):
        own = X.at[z]
        if i == 0:
            return to(tok_hbm.at[0, lo], own.at[lo], tok_s.at[0], tok_r.at[0], dz=1)
        if i == 1:
            return to(tok_hbm.at[0, hi], own.at[hi], tok_s.at[1], tok_r.at[1], dz=1)
        if i == 3:
            return to(tok_hbm.at[0, hi], own.at[hi], tok_s.at[3], tok_r.at[3], dz=-1)
        if i == 4:
            return to(tok_hbm.at[0, lo], own.at[lo], tok_s.at[4], tok_r.at[4], dz=-1)
        if i == 2:
            b = X.at[ring(z, -1), lo]
            return to(b, b, tok_s.at[2], tok_r.at[2], dz=1)
        b = X.at[ring(z, 1), hi]
        return to(b, b, tok_s.at[5], tok_r.at[5], dz=-1)

    def tok_in(i):
        src = {0: -1, 1: -1, 2: 2, 3: 1, 4: 1, 5: 2}[i]
        half = {0: lo, 1: hi, 2: lo, 3: hi, 4: lo, 5: hi}[i]
        b = X.at[ring(z, src), half]
        return to(b, b, tok_s.at[i], tok_r.at[i], dz=1)

    DY = (1, -1, 2)

    def wy(i):
        return to(wqkv_hbm, W.at[dp, y], wy_s.at[i], wy_r.at[i], dy=DY[i])

    def wy_in(i):
        b = W.at[dp, ring(y, -DY[i])]
        return to(b, b, wy_s.at[i], wy_r.at[i], dy=1)

    def wblk(r, dx):
        return W.at[ring(x, dx) * 2 + c, ring(y, r)]

    def wx(r, k):
        ss, rs = wx_s.at[r, k], wx_r.at[r, k]
        if k == 0 or k == 1:
            b = wblk(r, 0)
            return to(b, b, ss, rs, dx=1 if k == 0 else -1)
        if k == 2:
            b = wblk(r, -1).at[lo]
            return to(b, b, ss, rs, dx=1)
        b = wblk(r, 1).at[hi]
        return to(b, b, ss, rs, dx=-1)

    def wx_in(r, k):
        ss, rs = wx_s.at[r, k], wx_r.at[r, k]
        b = (wblk(r, -1), wblk(r, 1), wblk(r, 2).at[lo], wblk(r, 2).at[hi])[k]
        return to(b, b, ss, rs, dx=1)

    DXK = (0, -1, 1, 2)

    def wp(r, k):
        b = W.at[ring(x, DXK[k]) * 2 + c, ring(y, r)]
        return to(b, b, wp_s.at[r, k], wp_r.at[r, k], other=True)

    def wp_in(r, k):
        b = W.at[ring(x, DXK[k]) * 2 + (1 - c), ring(y, r)]
        return to(b, b, wp_s.at[r, k], wp_r.at[r, k], other=True)

    def oz(i):
        return to(wo_hbm, WO.at[dp, y, z], oz_s.at[i], oz_r.at[i], dz=DY[i])

    def oz_in(i):
        b = WO.at[dp, y, ring(z, -DY[i])]
        return to(b, b, oz_s.at[i], oz_r.at[i], dz=1)

    def oy(i):
        b = WO.at[dp, y]
        return to(b, b, oy_s.at[i], oy_r.at[i], dy=DY[i])

    def oy_in(i):
        b = WO.at[dp, ring(y, -DY[i])]
        return to(b, b, oy_s.at[i], oy_r.at[i], dy=1)

    y01, y23 = pl.ds(0, 2), pl.ds(2, 2)

    def ox(k):
        ss, rs = ox_s.at[k], ox_r.at[k]
        if k < 2:
            b = WO.at[dp]
            return to(b, b, ss, rs, dx=1 if k == 0 else -1)
        if k == 2:
            b = WO.at[ring(x, -1) * 2 + c, y01]
            return to(b, b, ss, rs, dx=1)
        b = WO.at[ring(x, 1) * 2 + c, y23]
        return to(b, b, ss, rs, dx=-1)

    def ox_in(k):
        far = ring(x, 2) * 2 + c
        b = (
            WO.at[ring(x, -1) * 2 + c], WO.at[ring(x, 1) * 2 + c],
            WO.at[far, y01], WO.at[far, y23],
        )[k]
        return to(b, b, ox_s.at[k], ox_r.at[k], dx=1)

    def op(k):
        b = WO.at[ring(x, DXK[k]) * 2 + c]
        return to(b, b, op_s.at[k], op_r.at[k], other=True)

    def op_in(k):
        b = WO.at[ring(x, DXK[k]) * 2 + (1 - c)]
        return to(b, b, op_s.at[k], op_r.at[k], other=True)

    def kvc(r, k):
        ss, rs = kv_s.at[r, k], kv_r.at[r, k]
        zz = ring(z, r)
        if k < 2:
            b = KVB.at[y * 4 + zz]
            return to(b, b, ss, rs, dy=1 if k == 0 else -1)
        if k == 2:
            b = KVB.at[ring(y, -1) * 4 + zz, 0]
            return to(b, b, ss, rs, dy=1)
        b = KVB.at[ring(y, 1) * 4 + zz, 1]
        return to(b, b, ss, rs, dy=-1)

    def kvc_in(r, k):
        zz = ring(z, r)
        b = (
            KVB.at[ring(y, -1) * 4 + zz], KVB.at[ring(y, 1) * 4 + zz],
            KVB.at[ring(y, 2) * 4 + zz, 0], KVB.at[ring(y, 2) * 4 + zz, 1],
        )[k]
        return to(b, b, kv_s.at[r, k], kv_r.at[r, k], dy=1)

    def at(r, h):
        return to(
            AO.at[r - 1, h], ATT.at[z, h], at_s.at[r - 1, h], at_r.at[r - 1, h], dz=r
        )

    def at_in(r, h):
        b = ATT.at[ring(z, -r), h]
        return to(b, b, at_s.at[r - 1, h], at_r.at[r - 1, h], dz=1)

    copy_x = pltpu.make_async_copy(tok_hbm.at[0], X.at[z], loc.at[0])
    copy_w = pltpu.make_async_copy(wqkv_hbm, W.at[dp, y], loc.at[1])
    copy_o = pltpu.make_async_copy(wo_hbm, WO.at[dp, y, z], loc.at[2])
    copy_w.start()
    for i in range(3):
        wy(i).start()
    tok(0).start()
    tok(3).start()
    copy_o.start()
    for i in range(3):
        oz(i).start()
    tok(1).start()
    tok(4).start()
    copy_x.start()

    copy_w.wait()
    for r in (0, 3, 1, 2):
        if r:
            wy_in({3: 0, 1: 1, 2: 2}[r]).wait_recv()
        wx(r, 0).start()
        wx(r, 1).start()
        wp(r, 0).start()
    copy_o.wait()
    for i in range(3):
        oz_in(i).wait_recv()
    for i in range(3):
        oy(i).start()
    for r in (0, 3, 1, 2):
        wx_in(r, 0).wait_recv()
        wx(r, 2).start()
        wp(r, 1).start()
        wx_in(r, 1).wait_recv()
        wx(r, 3).start()
        wp(r, 2).start()
        if r == 3:
            tok_in(0).wait_recv()
            tok(2).start()
            tok_in(3).wait_recv()
            tok(5).start()
    for i in range(3):
        oy_in(i).wait_recv()
    ox(0).start()
    ox(1).start()
    op(0).start()
    for r in (0, 3, 1, 2):
        wx_in(r, 2).wait_recv()
        wx_in(r, 3).wait_recv()
        wp(r, 3).start()
    for r in (0, 3, 1, 2):
        for k in range(4):
            wp_in(r, k).wait_recv()
    copy_x.wait()

    lane = lax.broadcasted_iota(jnp.int32, (64, HD), 1)
    low64 = lane < 64
    even = lane % 2 == 0

    def normed_turned(raw, gain, cosv, sin_a, sin_b):
        n = raw * lax.rsqrt(jnp.mean(raw * raw, axis=1, keepdims=True) + EPS) * gain
        return n * cosv + (pltpu.roll(n, HD - 1, 1) * sin_a + pltpu.roll(n, 1, 1) * sin_b)

    def project_slot(s, carry):
        r = s ^ (s >> 1)
        zz = lax.rem(z + r, 4)

        @pl.when(s == 1)
        def _():
            tok_in(3).wait_recv() if False else None
            tok_in(4).wait_recv()

        @pl.when(s == 2)
        def _():
            tok_in(1).wait_recv()

        @pl.when(s == 3)
        def _():
            tok_in(2).wait_recv()
            tok_in(5).wait_recv()

        chunk = y * 4 + zz
        first_row = (zz * 4 + y) * 4

        def one_kv_head(j, carry2):
            raws = []
            for b in range(2):
                raw = jnp.zeros((ROWS, ROWS), F32)
                for k in range(8):
                    raw = raw + jnp.dot(
                        X[zz, :, k * 256:(k + 1) * 256], W[k, 2 * j + b],
                        preferred_element_type=F32,
                    )
                raws.append(raw)
            gq = gain_ref[0:1, :]
            gk = gain_ref[1:2, :]
            for g in range(4):
                sl = slice(g * 64, (g + 1) * 64)
                crow = cos_ref[pl.ds(first_row + g, 1), :]
                srow = sin_ref[pl.ds(first_row + g, 1), :]
                cosv = jnp.where(low64, crow, cos_ref[...])
                sinv = jnp.where(low64, srow, sin_ref[...])
                sin_a = jnp.where(even, -sinv, 0.0)
                sin_b = jnp.where(even, 0.0, sinv)
                for b in range(2):
                    qn = normed_turned(raws[b][sl, 0:HD], gq, cosv, sin_a, sin_b)
                    S[b, sl, 0:HD] = qn
                a0 = raws[0][sl, HD:]
                a1 = raws[1][sl, HD:]
                kk = jnp.where(low64, a0, pltpu.roll(a1, 64, 1))
                vv = jnp.where(low64, pltpu.roll(a0, 64, 1), a1)
                kn = normed_turned(kk, gk, cosv, sin_a, sin_b)
                KVB[chunk, j, 0, sl, :] = kn.astype(BF)
                S[2, sl, 0:HD] = vv
            for b in range(2):
                for half in range(2):
                    hs = slice(half * 128, (half + 1) * 128)
                    QT[zz, 2 * j + b, :, hs] = S[b, hs, 0:HD].T.astype(BF)
            for half in range(2):
                hs = slice(half * 128, (half + 1) * 128)
                KVB[chunk, j, 1, hs, :] = S[2, hs, 0:HD].T.astype(BF)
            return carry2

        lax.fori_loop(0, 2, one_kv_head, 0)

        for r_static in range(4):
            @pl.when(r == r_static)
            def _():
                kvc(r_static, 0).start()
                kvc(r_static, 1).start()
        return carry

    lax.fori_loop(0, 4, project_slot, 0)

    for r in (0, 1, 3, 2):
        kvc_in(r, 0).wait_recv()
        kvc(r, 2).start()
        kvc_in(r, 1).wait_recv()
        kvc(r, 3).start()
    for r in (0, 1, 3, 2):
        kvc_in(r, 2).wait_recv()
        kvc_in(r, 3).wait_recv()

    cs = HD ** (-0.5) * math.log2(math.e)
    NEG = jnp.full((8, 256), -jnp.inf, F32)

    def tile_of(i):
        r = lax.rem(i // 4 + 1, 4)
        return r, lax.rem(z + r, 4), lax.rem(i, 4)

    def score_chunk(ck, kvh, qt, m8):
        s_new = jnp.dot(KVB[ck, kvh, 0], qt, preferred_element_type=F32)
        S[ck] = s_new
        return jnp.maximum(m8, jnp.max(s_new.reshape(32, 8, 256), axis=0))

    def first_scores(ck, m8):
        _, zz, h = tile_of(0)
        return score_chunk(ck, h // 2, QT[zz, h], m8)

    m_first = lax.fori_loop(0, 16, first_scores, NEG)

    def tile(i, m8):
        r, zz, h = tile_of(i)
        nxt = lax.rem(i + 1, 16)
        _, zn, hn = tile_of(nxt)
        kvh, kvn = h // 2, hn // 2
        mb = jnp.broadcast_to(jnp.max(m8, axis=0, keepdims=True), (8, 256))
        ACC[...] = jnp.zeros_like(ACC)

        def four(c4, carry):
            m_new, l8 = carry
            pv = None
            for j in range(4):
                ck = c4 * 4 + j
                p = jnp.exp2((S[ck].reshape(32, 8, 256) - mb[None]) * cs)
                l8 = l8 + jnp.sum(p, axis=0)
                vt = jnp.concatenate(
                    [KVB[ck, kvh, 1, 0:128, :], KVB[ck, kvh, 1, 128:256, :]], axis=1
                )
                d = jnp.dot(vt, p.reshape(256, 256).astype(BF), preferred_element_type=F32)
                pv = d if pv is None else pv + d
                m_new = score_chunk(ck, kvn, QT[zn, hn], m_new)
            ACC[...] += pv
            return m_new, l8

        m_new, l8 = lax.fori_loop(0, 4, four, (NEG, jnp.zeros((8, 256), F32)))
        inv = 1.0 / jnp.sum(l8, axis=0, keepdims=True)
        o = (ACC[...] * inv).T.astype(BF)

        @pl.when(r == 0)
        def _():
            ATT[z, h] = o

        for r_static in range(1, 4):
            @pl.when(r == r_static)
            def _():
                AO[r_static - 1, h] = o
                at(r_static, h).start()

        @pl.when(i == 6)
        def _():
            ox_in(0).wait_recv()
            ox(2).start()
            op(1).start()
            ox_in(1).wait_recv()
            ox(3).start()
            op(2).start()

        @pl.when(i == 13)
        def _():
            ox_in(2).wait_recv()
            ox_in(3).wait_recv()
            op(3).start()

        return m_new

    lax.fori_loop(0, 16, tile, m_first)

    for k in range(4):
        op_in(k).wait_recv()
    for r in range(1, 4):
        for h in range(4):
            at_in(r, h).wait_recv()

    def out_block(n, carry):
        zc, yc = n // 2, lax.rem(n, 2) * 2
        total = jnp.zeros((ROWS, 256), F32)
        for k in range(8):
            lhs = jnp.concatenate(
                [ATT[k // 2, 2 * (k % 2)], ATT[k // 2, 2 * (k % 2) + 1]], axis=1
            )
            rhs = jnp.concatenate([WO[k, yc, zc], WO[k, yc + 1, zc]], axis=1)
            total = total + jnp.dot(lhs, rhs, preferred_element_type=F32)
        out_ref[:, pl.ds(pl.multiple_of(n * 256, 256), 256)] = total.astype(BF)
        return carry

    lax.fori_loop(0, 8, out_block, 0)

    for i in range(6):
        tok(i).wait_send()
    for i in range(3):
        wy(i).wait_send()
        oz(i).wait_send()
        oy(i).wait_send()
    for r in range(4):
        for k in range(4):
            wx(r, k).wait_send()
            wp(r, k).wait_send()
            kvc(r, k).wait_send()
    for k in range(4):
        ox(k).wait_send()
        op(k).wait_send()
    for r in range(1, 4):
        for h in range(4):
            at(r, h).wait_send()


def on_device(tokens, w_query, w_key, w_value, w_out, qk_gain):
    wqkv = jnp.concatenate([w_query, w_key, w_value], axis=1)
    cos_t, sin_t = rope_tables()
    any_ = pl.BlockSpec(memory_space=pl.ANY)
    vm = pl.BlockSpec(memory_space=pltpu.VMEM)
    dma = pltpu.SemaphoreType.DMA
    out = pl.pallas_call(
        kernel,
        out_shape=jax.ShapeDtypeStruct((ROWS, 2048), BF),
        in_specs=[any_, any_, any_, vm, vm, vm],
        out_specs=vm,
        scratch_shapes=[
            pltpu.VMEM((4, ROWS, 2048), BF),
            pltpu.VMEM((8, 4, ROWS, 256), BF),
            pltpu.VMEM((8, 4, 4, ROWS, 128), BF),
            pltpu.VMEM((4, 4, HD, ROWS), BF),
            pltpu.VMEM((16, 2, 2, ROWS, HD), BF),
            pltpu.VMEM((16, ROWS, ROWS), F32),
            pltpu.VMEM((HD, ROWS), F32),
            pltpu.VMEM((3, 4, ROWS, HD), BF),
            pltpu.VMEM((4, 4, ROWS, HD), BF),
            dma((3,)),
            dma((6,)), dma((6,)),
            dma((3,)), dma((3,)),
            dma((4, 4)), dma((4, 4)),
            dma((4, 4)), dma((4, 4)),
            dma((3,)), dma((3,)),
            dma((3,)), dma((3,)),
            dma((4,)), dma((4,)),
            dma((4,)), dma((4,)),
            dma((4, 4)), dma((4, 4)),
            dma((3, 4)), dma((3, 4)),
        ],
        compiler_params=pltpu.CompilerParams(
            collective_id=0, has_side_effects=True, vmem_limit_bytes=56 * 1024 * 1024
        ),
    )(tokens, wqkv, w_out, qk_gain, jnp.asarray(cos_t), jnp.asarray(sin_t))
    return out[None]


def solution(mesh):
    in_specs = (
        P("dp", "sp", None),
        P("dp", "sp"),
        P("dp", "sp"),
        P("dp", "sp"),
        P("dp", "sp"),
        P(),
    )
    out_specs = P("dp", "sp", None)
    return jax.shard_map(
        on_device, mesh=mesh, in_specs=in_specs, out_specs=out_specs, check_vma=False
    )
```

time: 290 us -> 120 us (0.41)
  Pallas kernels: 0 us -> 114 us
  waiting for transfers between devices: 91.1 us -> 0 us
  blocking collectives: 69.9 us -> 0 us
  matrix products: 56.2 us -> 0 us
  other arithmetic: 22.9 us -> 0.75 us
  starting transfers between devices: 19.7 us -> 0 us
  between operations: 13.4 us -> 0.03 us
  local copies, waits for them, and re-layouts: 15.2 us -> 4.02 us
    pallas_call x0 -> x1, Pallas kernels: none -> 114 us  [on_device(): pl.pallas_call(kernel, out_shape=jax.ShapeDtypeStruct((ROWS, 2048), BF),...]
    all_to_all x4 -> x0, blocking collectives: 69.9 us -> none  [the longest x3 50 us: sent_to_all(): return lax.all_to_all(copies, axis, split_axis=0, concat_axis=0, tiled=True)]
    all_gather x4 -> x0, waiting for transfers between devices: 67.3 us -> none  [project(): lax.all_gather(col_full, 'dp', axis=0, tiled=True)]
    dot_general x20 -> x0, matrix products: 56.2 us -> none  [the longest x8 24.7 us: one_block(): jnp.dot(probs_bf, value_rows, preferred_element_type=jnp.float32)]
    all_to_all x4 -> x0, waiting for transfers between devices: 23.3 us -> none  [the longest x1 15.3 us: on_device(): lax.all_to_all(prepare(raw_proj, qk_gain[0], cosine, sine_table).reshape(...]
    all_to_all x4 -> x0, starting transfers between devices: 19.6 us -> none  [the longest x1 6.77 us: on_device(): lax.all_to_all(value_send, 'sp', split_axis=1, concat_axis=0, tiled=True)]
    reduce_sum x8 -> x0, other arithmetic: 12.1 us -> none  [one_block(): row_total = jnp.sum(weights, axis=1, keepdims=True)]
    another operation x4 -> x0, other arithmetic: 6.95 us -> none
  transfers between devices with their start and end apart: 8 -> 0, of which waited for: 5 -> 0; matrix products, arithmetic and copies ran while one was open for 30% -> 0% of each run, Pallas kernels for 0% -> 0%
where the time goes in v1:
time: 120 us; the launch traced here: 119 us
  Pallas kernels  114 us (95%)
  local copies, waits for them, and re-layouts  4.02 us (3%)
    pallas_call x1, Pallas kernels, on_device(): pl.pallas_call(kernel, out_shape=jax.ShapeDtypeStruct((ROWS, 2048), BF),...  114 us
    unnamed x7, local copies, waits for them, and re-layouts  4.02 us

profile of v1, /device:TPU:1, one launch (start us, length us, event | category | flops | bytes accessed | tf_op | source)
XLA Modules:
  0.0 119.3 jit_solution(6129540431446343670)
XLA Ops:
  0.0 0.0 copy-start.1
  0.0 0.9 copy.9
  0.9 0.0 copy-done.1
  0.9 0.0 copy-start
  0.9 0.1 copy.10
  1.0 0.7 copy-done
  1.7 0.7 pad_maximum_fusion.wqkv_hbm
  2.5 114.5 %shard_map.82 = bf16[256,2048]{1,0:T(8,128)(2,1)} custom-call(bf16[1,256,2048]{2,1,0:T(8,128)(2,1)} %tok_hbm.1, bf16[256,256]{1,0:T(8,128)(2,1)} %pad_maximum_fusion.wqkv_hbm, bf16[256,128]{1,0:T(8,128)(2,1)} %wo_hbm.1, f32[2,128]{1,0:T(2,128)} %gain_ref.1, f32[64,128]{1,0:T(8,128)} %constant.4.clone.cos_ref, f32[64,128]{1,0:T(8,128)} %constant.5.clone.sin_ref), custom_call_target="tpu_custom_call" | custom-call | tf_op jit(solution)/shard_map/pallas_call | solution.py:469
  117.0 2.3 %copy.12 = bf16[1,256,2048]{2,1,0:T(8,128)(2,1)} copy(bf16[1,256,2048]{2,1,0:T(8,128)(2,1)} %bitcast.1) | data formatting | bytes 2097152
Async XLA Ops:
  0.0 0.9 copy-start.1
  0.9 0.8 copy-start

commit v2 on v0

v2 whole, which is shorter than its diff:
```python
import functools
import math

import jax
import jax.numpy as jnp
import numpy as np
from jax import lax
from jax.experimental import pallas as pl
from jax.experimental.pallas import tpu as pltpu
from jax.sharding import PartitionSpec as P

HQ = 16
KV = 8
HD = 128
GRID_W = 64
ROPE_BASE = 10000.0
EPS = 1e-06
ROWS = 256
BF = jnp.bfloat16
F32 = jnp.float32


def rope_tables():
    quarter = np.arange(0, HD // 2, 2, dtype=np.float32)
    inv_freq = np.float32(ROPE_BASE) ** (-quarter / np.float32(HD // 2))
    angle = np.arange(GRID_W, dtype=np.float32)[:, None] * inv_freq.astype(np.float32)
    angle = np.repeat(angle, 2, axis=1).astype(np.float64)
    angle = np.concatenate([angle, angle], axis=1)
    return np.cos(angle).astype(np.float32), np.sin(angle).astype(np.float32)


class Ring:
    def __init__(self, copy, slot, half, step, send, recv):
        self.copy, self.slot, self.half, self.step = copy, slot, half, step
        self.send, self.recv = send, recv

    def out(self, k):
        if k == 0 or k == 1:
            block = self.slot(0)
        elif k == 2:
            block = self.half(self.slot(3), 0)
        else:
            block = self.half(self.slot(1), 1)
        return self.copy(block, block, self.send(k), self.recv(k), **self.step(1 if k % 2 == 0 else 3))

    def into(self, k):
        far = self.slot(2)
        block = (self.slot(3), self.slot(1), self.half(far, 0), self.half(far, 1))[k]
        return self.copy(block, block, self.send(k), self.recv(k), **self.step(1))


def kernel(
    tok_hbm, wq_hbm, wk_hbm, wv_hbm, wo_hbm, gain_ref, cos_ref, sin_ref,
    out_ref,
    X, W, WO, QT, KVB, S, ACC, MX, LS, AO, ATT,
    loc, tok_s, tok_r, w1_s, w1_r, w2_s, w2_r, wp_s, wp_r,
    oz_s, oz_r, oy_s, oy_r, ox_s, ox_r, op_s, op_r,
    kv_s, kv_r, at_s, at_r,
):
    sp = lax.axis_index("sp")
    dp = lax.axis_index("dp")
    z, y = sp // 4, sp % 4
    x, c = dp // 2, dp % 2

    def ring(v, d):
        return (v + d + 4) % 4

    def device(dz=0, dy=0, dx=0, other=False):
        return {
            "sp": ring(z, dz) * 4 + ring(y, dy),
            "dp": ring(x, dx) * 2 + ((1 - c) if other else c),
        }

    def to(src, dst, ss, rs, **where):
        return pltpu.make_async_remote_copy(
            src_ref=src, dst_ref=dst, send_sem=ss, recv_sem=rs,
            device_id=device(**where), device_id_type=pl.DeviceIdType.MESH,
        )

    lo, hi = pl.ds(0, 128), pl.ds(128, 128)

    local = [
        (wq_hbm, W.at[dp, y, 0]),
        (wk_hbm.at[:, lo], W.at[dp, y, 1, pl.ds(0, 64)]),
        (wk_hbm.at[:, hi], W.at[dp, y, 1, pl.ds(128, 64)]),
        (wv_hbm.at[:, lo], W.at[dp, y, 1, pl.ds(64, 64)]),
        (wv_hbm.at[:, hi], W.at[dp, y, 1, pl.ds(192, 64)]),
        (wo_hbm, WO.at[dp, y, z]),
        (tok_hbm.at[0], X.at[0]),
    ]
    local = [pltpu.make_async_copy(a, b, loc.at[i]) for i, (a, b) in enumerate(local)]
    for one in local:
        one.start()

    barrier = pltpu.get_barrier_semaphore()
    for where in (
        dict(dz=1), dict(dz=3), dict(dz=2), dict(dy=1), dict(dy=3), dict(dx=1), dict(dx=3),
        dict(other=True),
    ):
        pl.semaphore_signal(
            barrier, inc=1, device_id=device(**where), device_id_type=pl.DeviceIdType.MESH
        )
    pl.semaphore_wait(barrier, 8)

    def tok(i):
        dst = (X.at[1, lo], X.at[1, hi], X.at[2, hi], X.at[2, lo], X.at[3, lo], X.at[3, hi])[i]
        src = (
            tok_hbm.at[0, lo], tok_hbm.at[0, hi], tok_hbm.at[0, hi], tok_hbm.at[0, lo],
            X.at[1, lo], X.at[1, hi],
        )[i]
        return to(src, dst, tok_s.at[i], tok_r.at[i], dz=1 if i % 2 == 0 else 3)

    def set_off(v, half):
        gray = v ^ (v >> 1)
        return gray if half else (4 - gray) % 4

    def wslot(cc, d1, d2):
        return W.at[ring(x, d2 * (1 - cc) + d1 * cc) * 2 + cc, ring(y, d1 * (1 - cc) + d2 * cc)]

    first_half = lambda ref, i: ref.at[i]
    w1 = Ring(
        to, lambda d: wslot(c, d, 0), first_half, lambda d: dict(dy=d * (1 - c), dx=d * c),
        lambda k: w1_s.at[k], lambda k: w1_r.at[k],
    )
    w2 = [
        Ring(
            to, lambda d, r=r: wslot(c, r, d), first_half,
            lambda d: dict(dy=d * c, dx=d * (1 - c)),
            lambda k, r=r: w2_s.at[r, k], lambda k, r=r: w2_r.at[r, k],
        )
        for r in range(4)
    ]

    def wp(r, d):
        b = wslot(c, r, d)
        return to(b, b, wp_s.at[r, d], wp_r.at[r, d], other=True)

    def wp_in(r, d):
        b = wslot(1 - c, r, d)
        return to(b, b, wp_s.at[r, d], wp_r.at[r, d], other=True)

    def oz(d):
        return to(wo_hbm, WO.at[dp, y, z], oz_s.at[d - 1], oz_r.at[d - 1], dz=d)

    def oz_in(d):
        b = WO.at[dp, y, ring(z, -d)]
        return to(b, b, oz_s.at[d - 1], oz_r.at[d - 1], dz=1)

    two = lambda ref, i: ref.at[pl.ds(2 * i, 2)]
    oy = Ring(
        to, lambda d: WO.at[dp, ring(y, d)], two,
        lambda d: dict(dy=d), lambda k: oy_s.at[k], lambda k: oy_r.at[k],
    )
    ox = Ring(
        to, lambda d: WO.at[ring(x, d) * 2 + c], two,
        lambda d: dict(dx=d), lambda k: ox_s.at[k], lambda k: ox_r.at[k],
    )

    def op(d):
        b = WO.at[ring(x, d) * 2 + c]
        return to(b, b, op_s.at[d], op_r.at[d], other=True)

    def op_in(d):
        b = WO.at[ring(x, d) * 2 + (1 - c)]
        return to(b, b, op_s.at[d], op_r.at[d], other=True)

    def kvr(v):
        return Ring(
            to, lambda d: KVB.at[ring(y, d) * 4 + v], first_half, lambda d: dict(dy=d),
            lambda k: kv_s.at[v, k], lambda k: kv_r.at[v, k],
        )

    def at(v, h, half):
        rows = hi if half else lo
        return to(
            AO.at[v - 1, h, rows], ATT.at[z, h, rows],
            at_s.at[v - 1, h, half], at_r.at[v - 1, h, half], dz=set_off(v, half),
        )

    def at_in(v, h, half):
        b = ATT.at[ring(z, -set_off(v, half)), h, hi if half else lo]
        return to(b, b, at_s.at[v - 1, h, half], at_r.at[v - 1, h, half], dz=1)

    for d in (2, 1, 3):
        oz(d).start()
    for i in range(4):
        tok(i).start()
    for i in range(5):
        local[i].wait()
    w1.out(0).start()
    w1.out(1).start()
    w2[0].out(0).start()
    w2[0].out(1).start()
    wp(0, 0).start()
    ACC[...] = jnp.zeros_like(ACC)
    LS[...] = jnp.zeros_like(LS)
    MX[...] = jnp.full(MX.shape, -jnp.inf, F32)
    for r, k in ((3, 0), (1, 1)):
        w1.into(k).wait_recv()
        w1.out(k + 2).start()
        w2[r].out(0).start()
        w2[r].out(1).start()
        wp(r, 0).start()
    w1.into(2).wait_recv()
    w1.into(3).wait_recv()
    w2[2].out(0).start()
    w2[2].out(1).start()
    wp(2, 0).start()
    local[5].wait()
    for d in (1, 3, 2):
        oz_in(d).wait_recv()
    oy.out(0).start()
    oy.out(1).start()
    for r in (0, 3, 1, 2):
        for k in range(2):
            w2[r].into(k).wait_recv()
            w2[r].out(k + 2).start()
            wp(r, 3 if k == 0 else 1).start()
    for r in (0, 3, 1, 2):
        w2[r].into(2).wait_recv()
        w2[r].into(3).wait_recv()
        wp(r, 2).start()
    for i in range(2):
        tok(i).wait_recv()
        tok(i + 4).start()
    for k in range(2):
        oy.into(k).wait_recv()
        oy.out(k + 2).start()
    for r in (0, 3, 1, 2):
        for d in (0, 3, 1, 2):
            wp_in(r, d).wait_recv()
    local[6].wait()

    lane = lax.broadcasted_iota(jnp.int32, (64, HD), 1)
    low64 = lane < 64
    even = lane % 2 == 0

    def normed_turned(raw, gain, cosv, sin_a, sin_b):
        n = raw * lax.rsqrt(jnp.mean(raw * raw, axis=1, keepdims=True) + EPS) * gain
        return n * cosv + (pltpu.roll(n, HD - 1, 1) * sin_a + pltpu.roll(n, 1, 1) * sin_b)

    def project(v):
        chunk = y * 4 + v
        gq = gain_ref[0:1, :]
        gk = gain_ref[1:2, :]
        turns = []
        for g in range(4):
            row = (ring(z, set_off(v, g // 2)) * 4 + y) * 4 + g
            cosv = jnp.where(low64, cos_ref[pl.ds(row, 1), :], cos_ref[...])
            sinv = jnp.where(low64, sin_ref[pl.ds(row, 1), :], sin_ref[...])
            turns.append((cosv, jnp.where(even, -sinv, 0.0), jnp.where(even, 0.0, sinv)))
        for j in range(2):
            rawq = jnp.zeros((ROWS, ROWS), F32)
            rawkv = jnp.zeros((ROWS, ROWS), F32)
            for k in range(8):
                rows = X[v, :, k * 256:(k + 1) * 256]
                rq = jnp.concatenate([W[k, 2 * j, 0], W[k, 2 * j + 1, 0]], axis=1)
                rkv = jnp.concatenate(
                    [
                        jnp.concatenate([W[k, b, 1, 0:128], W[k, b, 1, 128:256]], axis=1)
                        for b in (2 * j, 2 * j + 1)
                    ],
                    axis=0,
                )
                rawq = rawq + jnp.dot(rows, rq, preferred_element_type=F32)
                rawkv = rawkv + lax.dot_general(
                    rows, rkv, (((1,), (1,)), ((), ())), preferred_element_type=F32
                )
            for g in range(4):
                sl = slice(g * 64, (g + 1) * 64)
                for b in range(2):
                    S[3 * j + b, sl, 0:HD] = normed_turned(
                        rawq[sl, b * HD:(b + 1) * HD], gq, *turns[g]
                    )
                a0 = rawkv[sl, 0:HD]
                a1 = rawkv[sl, HD:]
                kk = jnp.where(low64, a0, pltpu.roll(a1, 64, 1))
                KVB[chunk, j, 0, sl, :] = normed_turned(kk, gk, *turns[g]).astype(BF)
                S[3 * j + 2, sl, 0:HD] = jnp.where(low64, pltpu.roll(a0, 64, 1), a1)
            for half in range(2):
                hs = slice(half * 128, (half + 1) * 128)
                for b in range(2):
                    QT[v, 2 * j + b, :, hs] = S[3 * j + b, hs, 0:HD].T.astype(BF)
                KVB[chunk, j, 1, hs, :] = S[3 * j + 2, hs, 0:HD].T.astype(BF)

    def project_and_send(v, carry):
        project(v)
        ringv = kvr(v)
        ringv.out(0).start()
        ringv.out(1).start()
        return carry

    def kv_pass_on(v):
        ringv = kvr(v)
        for k in range(2):
            ringv.into(k).wait_recv()
            ringv.out(k + 2).start()

    def kv_far(v):
        ringv = kvr(v)
        ringv.into(2).wait_recv()
        ringv.into(3).wait_recv()

    cs = HD ** (-0.5) * math.log2(math.e)
    NEG = jnp.full((8, 256), -jnp.inf, F32)

    def run_units(n, unit_of, chunks, finish=None, events=()):
        refs = [ring(y, dy) * 4 + v for dy, v in chunks]

        def scores(u, j, m8):
            v, h = unit_of(u)
            s = jnp.dot(KVB[refs[j], h // 2, 0], QT[v, h], preferred_element_type=F32)
            S[j] = s
            return jnp.maximum(m8, jnp.max(s.reshape(32, 8, 256), axis=0))

        m8 = NEG
        for j in range(len(refs)):
            m8 = scores(0, j, m8)

        def unit(u, m8):
            v, h = unit_of(u)
            nxt = jnp.minimum(u + 1, n - 1)
            t = v * 4 + h
            m_old = MX[t]
            m = jnp.maximum(m_old, jnp.broadcast_to(jnp.max(m8, axis=0, keepdims=True), (8, 256)))
            alpha = jnp.exp2((m_old - m) * cs)
            l8 = LS[t] * alpha
            pv = None
            m_next = NEG
            for j in range(len(refs)):
                p = jnp.exp2((S[j].reshape(32, 8, 256) - m[None]) * cs)
                l8 = l8 + jnp.sum(p, axis=0)
                vt = jnp.concatenate(
                    [KVB[refs[j], h // 2, 1, 0:128, :], KVB[refs[j], h // 2, 1, 128:256, :]],
                    axis=1,
                )
                d = jnp.dot(vt, p.reshape(256, 256).astype(BF), preferred_element_type=F32)
                pv = d if pv is None else pv + d
                m_next = scores(nxt, j, m_next)
            acc = (ACC[t].reshape(16, 8, 256) * alpha[None]).reshape(HD, ROWS) + pv
            if finish is None:
                MX[t] = m
                LS[t] = l8
                ACC[t] = acc
            else:
                finish(v, h, acc * (1.0 / jnp.sum(l8, axis=0, keepdims=True)))
            for when, event in events:
                pl.when(u == when)(event)
            return m_next

        lax.fori_loop(0, n, unit, m8)

    def finish(v, h, o):
        rows = o.T.astype(BF)

        @pl.when(v == 0)
        def _():
            ATT[z, h] = rows

        @pl.when(v != 0)
        def _():
            AO[v - 1, h] = rows
            at(v, h, 0).start()
            at(v, h, 1).start()

    def ox_start():
        oy.into(2).wait_recv()
        oy.into(3).wait_recv()
        ox.out(0).start()
        ox.out(1).start()
        op(0).start()

    def ox_pass_on():
        for k in range(2):
            ox.into(k).wait_recv()
            ox.out(k + 2).start()
            op(3 if k == 0 else 1).start()

    def ox_far():
        ox.into(2).wait_recv()
        ox.into(3).wait_recv()
        op(2).start()

    lax.fori_loop(0, 2, project_and_send, 0)
    ox_start()
    tok(2).wait_recv()
    tok(3).wait_recv()
    project_and_send(2, 0)
    kv_pass_on(0)
    own3 = ((0, 0), (0, 1), (0, 2))
    near2 = ((1, 0), (3, 0), (1, 1), (3, 1))
    run_units(12, lambda u: (u // 4, u % 4), own3)
    kv_pass_on(1)
    run_units(12, lambda u: (u // 4, u % 4), near2)
    tok(4).wait_recv()
    tok(5).wait_recv()
    project_and_send(3, 0)
    kv_pass_on(2)
    run_units(4, lambda u: (3, u), own3 + near2)
    kv_far(0)
    kv_far(1)
    run_units(
        16, lambda u: (u // 4, u % 4), ((0, 3), (2, 0), (2, 1), (1, 2), (3, 2)),
        events=((10, lambda: kv_pass_on(3)), (12, ox_pass_on)),
    )
    kv_far(2)
    kv_far(3)
    run_units(
        16, lambda u: (3 - u // 4, u % 4), ((2, 2), (1, 3), (3, 3), (2, 3)),
        finish=finish, events=((14, ox_far),),
    )
    for v in range(1, 4):
        for h in range(4):
            for half in range(2):
                at_in(v, h, half).wait_recv()
    for d in (0, 3, 1, 2):
        op_in(d).wait_recv()

    def out_block(n, carry):
        zc, yc = n // 2, lax.rem(n, 2) * 2
        total = jnp.zeros((ROWS, 256), F32)
        for k in range(8):
            lhs = jnp.concatenate(
                [ATT[k // 2, 2 * (k % 2)], ATT[k // 2, 2 * (k % 2) + 1]], axis=1
            )
            rhs = jnp.concatenate([WO[k, yc, zc], WO[k, yc + 1, zc]], axis=1)
            total = total + jnp.dot(lhs, rhs, preferred_element_type=F32)
        out_ref[:, pl.ds(pl.multiple_of(n * 256, 256), 256)] = total.astype(BF)
        return carry

    lax.fori_loop(0, 8, out_block, 0)
    for i in range(6):
        tok(i).wait_send()
    for d in (1, 2, 3):
        oz(d).wait_send()
    for k in range(4):
        for stage in (w1, oy, ox, *w2, *[kvr(v) for v in range(4)]):
            stage.out(k).wait_send()
        op(k).wait_send()
        for r in range(4):
            wp(r, k).wait_send()
    for v in range(1, 4):
        for h in range(4):
            for half in range(2):
                at(v, h, half).wait_send()


def on_device(tokens, w_query, w_key, w_value, w_out, qk_gain):
    cos_t, sin_t = rope_tables()
    any_ = pl.BlockSpec(memory_space=pl.ANY)
    vm = pl.BlockSpec(memory_space=pltpu.VMEM)
    dma = pltpu.SemaphoreType.DMA
    pair = lambda *shape: [dma(shape), dma(shape)]
    out = pl.pallas_call(
        kernel,
        out_shape=jax.ShapeDtypeStruct((ROWS, 2048), BF),
        in_specs=[any_, any_, any_, any_, any_, vm, vm, vm],
        out_specs=vm,
        scratch_shapes=[
            pltpu.VMEM((4, ROWS, 2048), BF),
            pltpu.VMEM((8, 4, 2, ROWS, HD), BF),
            pltpu.VMEM((8, 4, 4, ROWS, HD), BF),
            pltpu.VMEM((4, 4, HD, ROWS), BF),
            pltpu.VMEM((16, 2, 2, ROWS, HD), BF),
            pltpu.VMEM((7, ROWS, ROWS), F32),
            pltpu.VMEM((16, HD, ROWS), F32),
            pltpu.VMEM((16, 8, ROWS), F32),
            pltpu.VMEM((16, 8, ROWS), F32),
            pltpu.VMEM((3, 4, ROWS, HD), BF),
            pltpu.VMEM((4, 4, ROWS, HD), BF),
            dma((7,)),
            *pair(6), *pair(4), *pair(4, 4), *pair(4, 4),
            *pair(3), *pair(4), *pair(4), *pair(4),
            *pair(4, 4), *pair(3, 4, 2),
        ],
        compiler_params=pltpu.CompilerParams(
            collective_id=0, has_side_effects=True, vmem_limit_bytes=56 * 1024 * 1024
        ),
    )(tokens, w_query, w_key.T, w_value.T, w_out, qk_gain, jnp.asarray(cos_t), jnp.asarray(sin_t))
    return out[None]


def solution(mesh):
    in_specs = (
        P("dp", "sp", None),
        P("dp", "sp"),
        P("dp", "sp"),
        P("dp", "sp"),
        P("dp", "sp"),
        P(),
    )
    out_specs = P("dp", "sp", None)
    return jax.shard_map(
        on_device, mesh=mesh, in_specs=in_specs, out_specs=out_specs, check_vma=False
    )
```

time: 290 us -> 88.3 us (0.30)
  waiting for transfers between devices: 91.1 us -> 0 us
  Pallas kernels: 0 us -> 85.7 us
  blocking collectives: 69.9 us -> 0 us
  matrix products: 56.2 us -> 0 us
  other arithmetic: 22.9 us -> 0 us
  starting transfers between devices: 19.7 us -> 0 us
  between operations: 13.4 us -> 0.01 us
  local copies, waits for them, and re-layouts: 15.2 us -> 2.3 us
    pallas_call x0 -> x1, Pallas kernels: none -> 85.7 us  [on_device(): pl.pallas_call(kernel, out_shape=jax.ShapeDtypeStruct((ROWS, 2048), BF),...]
    all_to_all x4 -> x0, blocking collectives: 69.9 us -> none  [the longest x3 50 us: sent_to_all(): return lax.all_to_all(copies, axis, split_axis=0, concat_axis=0, tiled=True)]
    all_gather x4 -> x0, waiting for transfers between devices: 67.3 us -> none  [project(): lax.all_gather(col_full, 'dp', axis=0, tiled=True)]
    dot_general x20 -> x0, matrix products: 56.2 us -> none  [the longest x8 24.7 us: one_block(): jnp.dot(probs_bf, value_rows, preferred_element_type=jnp.float32)]
    all_to_all x4 -> x0, waiting for transfers between devices: 23.3 us -> none  [the longest x1 15.3 us: on_device(): lax.all_to_all(prepare(raw_proj, qk_gain[0], cosine, sine_table).reshape(...]
    all_to_all x4 -> x0, starting transfers between devices: 19.6 us -> none  [the longest x1 6.77 us: on_device(): lax.all_to_all(value_send, 'sp', split_axis=1, concat_axis=0, tiled=True)]
    reduce_sum x8 -> x0, other arithmetic: 12.1 us -> none  [one_block(): row_total = jnp.sum(weights, axis=1, keepdims=True)]
    another operation x4 -> x0, other arithmetic: 6.95 us -> none
  transfers between devices with their start and end apart: 8 -> 0, of which waited for: 5 -> 0; matrix products, arithmetic and copies ran while one was open for 30% -> 0% of each run, Pallas kernels for 0% -> 0%
where the time goes in v2:
time: 88.3 us; the launch traced here: 88 us
  Pallas kernels  85.7 us (97%)
  local copies, waits for them, and re-layouts  2.3 us (3%)
    pallas_call x1, Pallas kernels, on_device(): pl.pallas_call(kernel, out_shape=jax.ShapeDtypeStruct((ROWS, 2048), BF),...  85.7 us
    unnamed x1, local copies, waits for them, and re-layouts  2.3 us

profile of v2, /device:TPU:1, one launch (start us, length us, event | category | flops | bytes accessed | tf_op | source)
XLA Modules:
  0.0 88.0 jit_solution(2094906915395993846)
XLA Ops:
  0.0 85.7 %shard_map.82 = bf16[256,2048]{1,0:T(8,128)(2,1)} custom-call(bf16[1,256,2048]{2,1,0:T(8,128)(2,1)} %tok_hbm.1, bf16[256,128]{1,0:T(8,128)(2,1)} %wq_hbm.1, bf16[64,256]{1,0:T(8,128)(2,1)} %bitcast.4, bf16[64,256]{1,0:T(8,128)(2,1)} %bitcast.5, bf16[256,128]{1,0:T(8,128)(2,1)} %wo_hbm.1, f32[2,128]{1,0:T(2,128)} %gain_ref.1, ...), custom_call_target="tpu_custom_call" | custom-call | tf_op jit(solution)/shard_map/pallas_call | solution.py:454
  85.7 2.3 %copy.10 = bf16[1,256,2048]{2,1,0:T(8,128)(2,1)} copy(bf16[1,256,2048]{2,1,0:T(8,128)(2,1)} %bitcast.3) | data formatting | bytes 2097152

commit v3 on v2

v3 whole, which is shorter than its diff:
```python
import functools
import math

import jax
import jax.numpy as jnp
import numpy as np
from jax import lax
from jax.experimental import pallas as pl
from jax.experimental.pallas import tpu as pltpu
from jax.sharding import PartitionSpec as P

HQ = 16
KV = 8
HD = 128
GRID_W = 64
ROPE_BASE = 10000.0
EPS = 1e-06
ROWS = 256
BF = jnp.bfloat16
F32 = jnp.float32


def rope_tables():
    quarter = np.arange(0, HD // 2, 2, dtype=np.float32)
    inv_freq = np.float32(ROPE_BASE) ** (-quarter / np.float32(HD // 2))
    angle = np.arange(GRID_W, dtype=np.float32)[:, None] * inv_freq.astype(np.float32)
    angle = np.repeat(angle, 2, axis=1).astype(np.float64)
    angle = np.concatenate([angle, angle], axis=1)
    return np.cos(angle).astype(np.float32), np.sin(angle).astype(np.float32)


class Ring:
    def __init__(self, copy, slot, half, step, send, recv):
        self.copy, self.slot, self.half, self.step = copy, slot, half, step
        self.send, self.recv = send, recv

    def out(self, k):
        if k == 0 or k == 1:
            block = self.slot(0)
        elif k == 2:
            block = self.half(self.slot(3), 0)
        else:
            block = self.half(self.slot(1), 1)
        return self.copy(block, block, self.send(k), self.recv(k), **self.step(1 if k % 2 == 0 else 3))

    def into(self, k):
        far = self.slot(2)
        block = (self.slot(3), self.slot(1), self.half(far, 0), self.half(far, 1))[k]
        return self.copy(block, block, self.send(k), self.recv(k), **self.step(1))


def kernel(
    tok_hbm, wq_hbm, wk_hbm, wv_hbm, wo_hbm, gain_ref, cos_ref, sin_ref,
    out_ref,
    X, W, WO, QT, KVB, S, ACC, MX, LS, AO, ATT, RB, OF, OB,
    loc, tok_s, tok_r, w1_s, w1_r, w2_s, w2_r, wp_s, wp_r,
    o1_s, o1_r, o2_s, o2_r, o3_s, o3_r, op_s, op_r,
    kv_s, kv_r, at_s, at_r, rl_s, rl_r, out_s,
):
    sp = lax.axis_index("sp")
    dp = lax.axis_index("dp")
    z, y = sp // 4, sp % 4
    x, c = dp // 2, dp % 2

    def ring(v, d):
        return (v + d + 4) % 4

    def device(dz=0, dy=0, dx=0, other=False):
        return {
            "sp": ring(z, dz) * 4 + ring(y, dy),
            "dp": ring(x, dx) * 2 + ((1 - c) if other else c),
        }

    def to(src, dst, ss, rs, **where):
        return pltpu.make_async_remote_copy(
            src_ref=src, dst_ref=dst, send_sem=ss, recv_sem=rs,
            device_id=device(**where), device_id_type=pl.DeviceIdType.MESH,
        )

    lo, hi = pl.ds(0, 128), pl.ds(128, 128)

    local = [
        (wq_hbm, W.at[dp, y, 0]),
        (wk_hbm.at[:, lo], W.at[dp, y, 1, pl.ds(0, 64)]),
        (wk_hbm.at[:, hi], W.at[dp, y, 1, pl.ds(128, 64)]),
        (wv_hbm.at[:, lo], W.at[dp, y, 1, pl.ds(64, 64)]),
        (wv_hbm.at[:, hi], W.at[dp, y, 1, pl.ds(192, 64)]),
        (wo_hbm, WO.at[c, x, y, z]),
        (tok_hbm.at[0], X.at[0]),
    ]
    local = [pltpu.make_async_copy(a, b, loc.at[i]) for i, (a, b) in enumerate(local)]
    for one in local:
        one.start()

    barrier = pltpu.get_barrier_semaphore()
    for where in (
        dict(dz=1), dict(dz=3), dict(dz=2), dict(dy=1), dict(dy=3), dict(dy=2), dict(dx=1),
        dict(dx=3), dict(dx=2), dict(other=True),
    ):
        pl.semaphore_signal(
            barrier, inc=1, device_id=device(**where), device_id_type=pl.DeviceIdType.MESH
        )
    pl.semaphore_wait(barrier, 10)

    def tok(i):
        dst = (X.at[1, lo], X.at[1, hi], X.at[2, hi], X.at[2, lo], X.at[3, lo], X.at[3, hi])[i]
        src = (
            tok_hbm.at[0, lo], tok_hbm.at[0, hi], tok_hbm.at[0, hi], tok_hbm.at[0, lo],
            X.at[1, lo], X.at[1, hi],
        )[i]
        return to(src, dst, tok_s.at[i], tok_r.at[i], dz=1 if i % 2 == 0 else 3)

    def set_off(v, half):
        gray = v ^ (v >> 1)
        return gray if half else (4 - gray) % 4

    def wslot(cc, d1, d2, part):
        cc1 = cc * part
        return W.at[
            ring(x, d2 * (1 - cc1) + d1 * cc1) * 2 + cc, ring(y, d1 * (1 - cc1) + d2 * cc1), part
        ]

    first_half = lambda ref, i: ref.at[i]
    row_half = lambda ref, i: ref.at[hi if i else lo]
    w1 = [
        Ring(
            to, lambda d, p=p: wslot(c, d, 0, p), row_half,
            lambda d, p=p: dict(dy=d * (1 - c * p), dx=d * c * p),
            lambda k, p=p: w1_s.at[p, k], lambda k, p=p: w1_r.at[p, k],
        )
        for p in range(2)
    ]
    w2 = [
        [
            Ring(
                to, lambda d, r=r, p=p: wslot(c, r, d, p), row_half,
                lambda d, p=p: dict(dy=d * c * p, dx=d * (1 - c * p)),
                lambda k, r=r, p=p: w2_s.at[p, r, k], lambda k, r=r, p=p: w2_r.at[p, r, k],
            )
            for r in range(4)
        ]
        for p in range(2)
    ]

    def wp(p, r, d):
        b = wslot(c, r, d, p)
        return to(b, b, wp_s.at[p, r, d], wp_r.at[p, r, d], other=True)

    def wp_in(p, r, d):
        b = wslot(1 - c, r, d, p)
        return to(b, b, wp_s.at[p, r, d], wp_r.at[p, r, d], other=True)

    oa, ob, oc = x, y, z

    def o1(d):
        return to(
            wo_hbm, WO.at[c, oa, ob, oc], o1_s.at[d - 1], o1_r.at[d - 1], dz=d
        )

    def o1_in(d):
        b = WO.at[c, oa, ob, ring(oc, -d)]
        return to(b, b, o1_s.at[d - 1], o1_r.at[d - 1], dz=1)

    two = lambda ref, i: ref.at[pl.ds(2 * i, 2)]
    o2 = Ring(
        to, lambda d: WO.at[c, oa, ring(ob, d)], two,
        lambda d: dict(dy=d), lambda k: o2_s.at[k], lambda k: o2_r.at[k],
    )
    o3 = [
        Ring(
            to, lambda d, r=r: WO.at[c, ring(oa, d), ring(ob, r)], two,
            lambda d: dict(dx=d), lambda k, r=r: o3_s.at[r, k], lambda k, r=r: o3_r.at[r, k],
        )
        for r in range(4)
    ]

    def op(r, d):
        b = WO.at[c, ring(oa, d), ring(ob, r)]
        return to(b, b, op_s.at[r, d], op_r.at[r, d], other=True)

    def op_in(r, d):
        b = WO.at[1 - c, ring(oa, d), ring(y, r)]
        return to(b, b, op_s.at[r, d], op_r.at[r, d], other=True)

    def kvc(v, i, landing=False):
        half = (0, 1, 1, 0, 0, 1)[i]
        from_y = ((3, 3, 1, 1, 2, 2) if landing else (0, 0, 0, 0, 3, 1))[i]
        b = KVB.at[ring(y, from_y) * 4 + v, half]
        return to(b, b, kv_s.at[v, i], kv_r.at[v, i], dy=(1, 1, 3, 3, 1, 3)[i])

    def at(v, g, half):
        rows, heads = hi if half else lo, pl.ds(2 * g, 2)
        return to(
            AO.at[v, heads, rows], ATT.at[z, heads, rows],
            at_s.at[v - 1, g, half], at_r.at[v - 1, g, half], dz=set_off(v, half),
        )

    def at_in(v, g, half):
        b = ATT.at[ring(z, -set_off(v, half)), pl.ds(2 * g, 2), hi if half else lo]
        return to(b, b, at_s.at[v - 1, g, half], at_r.at[v - 1, g, half], dz=1)

    def relay_in(g, half):
        heads = pl.ds(2 * g, 2)
        return to(
            AO.at[3, heads, hi if half else lo], RB.at[half, heads],
            rl_s.at[g, half], rl_r.at[g, half], dz=3 if half else 1,
        )

    def relay_out(g, half):
        heads = pl.ds(2 * g, 2)
        return to(
            RB.at[half, heads], ATT.at[ring(z, 1 if half else 3), heads, hi if half else lo],
            at_s.at[2, g, half], at_r.at[2, g, half], dz=3 if half else 1,
        )

    def w1_near(p):
        for k in range(2):
            w1[p].into(k).wait_recv()
            if p == 0:
                w1[p].out(k + 2).start()

    def w1_far(p):
        if p == 0:
            w1[p].into(2).wait_recv()
            w1[p].into(3).wait_recv()
        else:
            w1_across(True).wait_recv()

    def w1_across(landing=False):
        b = wslot(c, 2 if landing else 0, 0, 1)
        return to(b, b, w1_s.at[1, 2], w1_r.at[1, 2], dy=2 * (1 - c), dx=2 * c)

    def w2_send(p, r):
        w2[p][r].out(0).start()
        w2[p][r].out(1).start()
        wp(p, r, 0).start()

    def w2_near(p, r):
        for k in range(2):
            w2[p][r].into(k).wait_recv()
            w2[p][r].out(k + 2).start()
            wp(p, r, 3 if k == 0 else 1).start()

    def w2_far(p, r):
        w2[p][r].into(2).wait_recv()
        w2[p][r].into(3).wait_recv()
        wp(p, r, 2).start()

    def wp_wait(p):
        for r in (0, 3, 1, 2):
            for d in (0, 3, 1, 2):
                wp_in(p, r, d).wait_recv()

    for d in (2, 1, 3):
        o1(d).start()
    for i in range(4):
        tok(i).start()
    for i in range(4):
        local[i + 1].wait()
    w1[1].out(0).start()
    w1[1].out(1).start()
    w1_across().start()
    local[0].wait()
    w1[0].out(0).start()
    w1[0].out(1).start()
    ACC[...] = jnp.zeros_like(ACC)
    LS[...] = jnp.zeros_like(LS)
    MX[...] = jnp.full(MX.shape, -jnp.inf, F32)
    def o3_send(r):
        o3[r].out(0).start()
        o3[r].out(1).start()
        op(r, 0).start()

    def o2_send():
        local[5].wait()
        for d in (1, 3, 2):
            o1_in(d).wait_recv()
        o2.out(0).start()
        o2.out(1).start()

    def o2_pass_on():
        for k in range(2):
            o2.into(k).wait_recv()
            o2.out(k + 2).start()
            o3_send(3 if k == 0 else 1)

    order = (0, 3, 1, 2)
    w1_near(1)
    for r in order[:3]:
        w2_send(1, r)
    w1_far(1)
    w2_send(1, 2)
    w1_near(0)
    pl.when(c == 0)(o2_send)
    for r in order:
        w2_near(1, r)
    w1_far(0)
    for r in order:
        w2_send(0, r)
    pl.when(c == 1)(o2_send)
    for r in order:
        w2_far(1, r)
    wp_wait(1)
    local[6].wait()
    lane = lax.broadcasted_iota(jnp.int32, (64, HD), 1)
    low64 = lane < 64
    even = lane % 2 == 0

    def normed_turned(raw, gain, cosv, sin_a, sin_b):
        n = raw * lax.rsqrt(jnp.mean(raw * raw, axis=1, keepdims=True) + EPS) * gain
        return n * cosv + (pltpu.roll(n, HD - 1, 1) * sin_a + pltpu.roll(n, 1, 1) * sin_b)

    def turns_of(v):
        turns = []
        for g in range(4):
            row = (ring(z, set_off(v, g // 2)) * 4 + y) * 4 + g
            cosv = jnp.where(low64, cos_ref[pl.ds(row, 1), :], cos_ref[...])
            sinv = jnp.where(low64, sin_ref[pl.ds(row, 1), :], sin_ref[...])
            turns.append((cosv, jnp.where(even, -sinv, 0.0), jnp.where(even, 0.0, sinv)))
        return turns

    def project_q(v):
        gq = gain_ref[0:1, :]
        turns = turns_of(v)
        for j in range(2):
            raw = jnp.zeros((ROWS, ROWS), F32)
            for k in range(8):
                rq = jnp.concatenate([W[k, 2 * j, 0], W[k, 2 * j + 1, 0]], axis=1)
                raw = raw + jnp.dot(
                    X[v, :, k * 256:(k + 1) * 256], rq, preferred_element_type=F32
                )
            for g in range(4):
                sl = slice(g * 64, (g + 1) * 64)
                for b in range(2):
                    S[j, b, sl, 0:HD] = normed_turned(
                        raw[sl, b * HD:(b + 1) * HD], gq, *turns[g]
                    )
            for half in range(2):
                hs = slice(half * 128, (half + 1) * 128)
                for b in range(2):
                    QT[v, 2 * j + b, :, hs] = S[j, b, hs, 0:HD].T.astype(BF)

    def project_kv(v):
        chunk = y * 4 + v
        gk = gain_ref[1:2, :]
        turns = turns_of(v)
        for j in range(2):
            raw = jnp.zeros((ROWS, ROWS), F32)
            for k in range(8):
                rkv = jnp.concatenate(
                    [
                        jnp.concatenate([W[k, b, 1, 0:128], W[k, b, 1, 128:256]], axis=1)
                        for b in (2 * j, 2 * j + 1)
                    ],
                    axis=0,
                )
                raw = raw + lax.dot_general(
                    X[v, :, k * 256:(k + 1) * 256], rkv, (((1,), (1,)), ((), ())),
                    preferred_element_type=F32,
                )
            for g in range(4):
                sl = slice(g * 64, (g + 1) * 64)
                a0 = raw[sl, 0:HD]
                a1 = raw[sl, HD:]
                kk = jnp.where(low64, a0, pltpu.roll(a1, 64, 1))
                KVB[chunk, j, 0, sl, :] = normed_turned(kk, gk, *turns[g]).astype(BF)
                S[j, 2, sl, 0:HD] = jnp.where(low64, pltpu.roll(a0, 64, 1), a1)
            for half in range(2):
                hs = slice(half * 128, (half + 1) * 128)
                KVB[chunk, j, 1, hs, :] = S[j, 2, hs, 0:HD].T.astype(BF)

    def kv_and_send(v):
        project_kv(v)
        for i in (0, 2, 1, 3):
            kvc(v, i).start()

    def kv_pass_on(v):
        for i in (0, 2):
            kvc(v, i, True).wait_recv()
            kvc(v, 4 + i // 2).start()

    def kv_near(v):
        for i in (1, 3):
            kvc(v, i, True).wait_recv()

    def kv_far(v):
        for i in (4, 5):
            kvc(v, i, True).wait_recv()

    cs = HD ** (-0.5) * math.log2(math.e)
    NEG = jnp.full((8, 256), -jnp.inf, F32)

    def run_units(n, unit_of, chunks, finish=None, events=()):
        refs = [ring(y, dy) * 4 + v for dy, v in chunks]

        def scores(u, j, b, m8):
            v, g = unit_of(u)
            s = jnp.dot(KVB[refs[j], g, 0], QT[v, 2 * g + b], preferred_element_type=F32)
            S[b, j] = s
            return jnp.maximum(m8, jnp.max(s.reshape(32, 8, 256), axis=0))

        def unit(u, m8s, more):
            v, g = unit_of(u)
            news = [NEG, NEG]
            for b in range(2):
                t = v * 4 + 2 * g + b
                m_old = MX[t]
                m = jnp.maximum(
                    m_old, jnp.broadcast_to(jnp.max(m8s[b], axis=0, keepdims=True), (8, 256))
                )
                alpha = jnp.exp2((m_old - m) * cs)
                l8 = LS[t] * alpha
                pv = None
                for j in range(len(refs)):
                    p = jnp.exp2((S[b, j].reshape(32, 8, 256) - m[None]) * cs)
                    l8 = l8 + jnp.sum(p, axis=0)
                    vt = jnp.concatenate(
                        [KVB[refs[j], g, 1, 0:128, :], KVB[refs[j], g, 1, 128:256, :]], axis=1
                    )
                    d = jnp.dot(vt, p.reshape(256, 256).astype(BF), preferred_element_type=F32)
                    pv = d if pv is None else pv + d
                    if more:
                        news[b] = scores(u + 1, j, b, news[b])
                acc = (ACC[t].reshape(16, 8, 256) * alpha[None]).reshape(HD, ROWS) + pv
                if finish is None:
                    MX[t] = m
                    LS[t] = l8
                    ACC[t] = acc
                else:
                    o = acc * (1.0 / jnp.sum(l8, axis=0, keepdims=True))
                    AO[v, 2 * g + b] = o.astype(BF).T
            if finish is not None:
                finish(v, g)
            return tuple(news)

        m8s = [NEG, NEG]
        for j in range(len(refs)):
            for b in range(2):
                m8s[b] = scores(0, j, b, m8s[b])

        def step(u, m8s):
            m8s = unit(u, m8s, True)
            for when, event in events:
                pl.when(u == when)(event)
            return m8s

        unit(n - 1, lax.fori_loop(0, n - 1, step, tuple(m8s)), False)

    def finish(v, g):
        @pl.when(v != 3)
        def _():
            @pl.when(v != 0)
            def _():
                at(v, g, 0).start()
                at(v, g, 1).start()

        @pl.when(v == 3)
        def _():
            relay_in(g, 0).start()
            relay_in(g, 1).start()

    def o2_far():
        o2.into(2).wait_recv()
        o2.into(3).wait_recv()
        o3_send(2)

    def o3_pass_on(*rs):
        for r in rs:
            for k in range(2):
                o3[r].into(k).wait_recv()
                o3[r].out(k + 2).start()
                op(r, 3 if k == 0 else 1).start()

    def o3_far(*rs):
        for r in rs:
            o3[r].into(2).wait_recv()
            o3[r].into(3).wait_recv()
            op(r, 2).start()

    def q_step(v, carry):
        project_q(v)
        return carry

    kv_and_send(0)
    for r in order:
        w2_near(0, r)
    o3_send(0)
    for i in range(2):
        tok(i).wait_recv()
        tok(i + 4).start()
    kv_and_send(1)
    o2_pass_on()
    for r in order:
        w2_far(0, r)
    wp_wait(0)
    lax.fori_loop(0, 2, q_step, 0)
    first_two = lambda u: (u // 2, u % 2)
    set_a = ((0, 0), (0, 1))
    set_b = ((0, 2), (1, 0), (3, 0))
    set_d = ((2, 0), (1, 1), (3, 1))
    run_units(4, first_two, set_a)
    kv_pass_on(0)
    kv_near(0)
    tok(2).wait_recv()
    tok(3).wait_recv()
    kv_and_send(2)
    project_q(2)
    run_units(4, first_two, set_b)
    run_units(2, lambda u: (2, u), set_a + set_b)
    o2_far()
    kv_pass_on(1)
    kv_near(1)
    kv_far(0)
    o3_pass_on(0)
    o3_pass_on(3)
    run_units(6, first_two, set_d)
    tok(4).wait_recv()
    tok(5).wait_recv()
    kv_and_send(3)
    project_q(3)
    run_units(2, lambda u: (3, u), set_a + set_b + set_d)
    kv_pass_on(2)
    kv_near(2)
    kv_far(1)

    run_units(
        8, first_two, ((0, 3), (2, 1), (1, 2), (3, 2)),
        events=(
            (0, lambda: o3_pass_on(1, 2)),
            (2, lambda: kv_pass_on(3)),
            (5, lambda: o3_far(0, 3)),
        ),
    )
    kv_far(2)
    kv_near(3)
    kv_far(3)

    def relay(g):
        for half in range(2):
            relay_in(g, half).wait_recv()
            relay_out(g, half).start()

    last = ((2, 2), (1, 3), (3, 3), (2, 3))
    run_units(4, lambda u: (3 - u, 0), last, finish=finish)
    run_units(
        4, lambda u: (3 - u, 1), last, finish=finish,
        events=((0, lambda: o3_far(1, 2)), (1, lambda: relay(0))),
    )
    relay(1)
    def out_terms(n, who):
        zc, yc = n // 2, (n % 2) * 2
        total = None
        for r in who:
            zs = ring(z, r)
            for i in range(2):
                src = AO.at[0] if r == 0 else ATT.at[zs]
                lhs = jnp.concatenate([src[2 * i], src[2 * i + 1]], axis=1)
                cols = [WO[i, zs, yc, zc], WO[i, zs, yc + 1, zc]]
                d = jnp.dot(lhs, jnp.concatenate(cols, axis=1), preferred_element_type=F32)
                total = d if total is None else total + d
        return total

    def own_block(zc, carry):
        for half in range(2):
            OF[2 * zc + half] = out_terms(2 * zc + half, (0,))
        return carry

    def out_copy(zc):
        cols = pl.ds(pl.multiple_of(zc * 512, 512), 512)
        return pltpu.make_async_copy(OB.at[zc], out_ref.at[:, cols], out_s.at[zc])

    def out_block(zc, carry):
        for half in range(2):
            total = OF[2 * zc + half] + out_terms(2 * zc + half, (1, 3, 2))
            OB[zc, :, half * 256:(half + 1) * 256] = total.astype(BF)
        out_copy(zc).start()
        return carry

    for r in range(4):
        for d in range(4):
            op_in(r, d).wait_recv()
    lax.fori_loop(0, 4, own_block, 0)
    for v in range(1, 4):
        for g in range(2):
            for half in range(2):
                at_in(v, g, half).wait_recv()
    lax.fori_loop(0, 4, out_block, 0)
    for i in range(6):
        tok(i).wait_send()
    for d in (1, 2, 3):
        o1(d).wait_send()
    w1[1].out(0).wait_send()
    w1[1].out(1).wait_send()
    w1_across().wait_send()
    for k in range(4):
        for stage in (w1[0], o2, *o3, *w2[0], *w2[1]):
            stage.out(k).wait_send()
        for r in range(4):
            op(r, k).wait_send()
            wp(0, r, k).wait_send()
            wp(1, r, k).wait_send()
    for v in range(4):
        for i in range(6):
            kvc(v, i).wait_send()
    for v in range(1, 4):
        for g in range(2):
            for half in range(2):
                (relay_out if v == 3 else functools.partial(at, v))(g, half).wait_send()
    for g in range(2):
        for half in range(2):
            relay_in(g, half).wait_send()
    for n in range(4):
        out_copy(n).wait()


def on_device(tokens, w_query, w_key, w_value, w_out, qk_gain):
    cos_t, sin_t = rope_tables()
    any_ = pl.BlockSpec(memory_space=pl.ANY)
    vm = pl.BlockSpec(memory_space=pltpu.VMEM)
    dma = pltpu.SemaphoreType.DMA
    pair = lambda *shape: [dma(shape), dma(shape)]
    out = pl.pallas_call(
        kernel,
        out_shape=jax.ShapeDtypeStruct((ROWS, 2048), BF),
        in_specs=[any_, any_, any_, any_, any_, vm, vm, vm],
        out_specs=any_,
        scratch_shapes=[
            pltpu.VMEM((4, ROWS, 2048), BF),
            pltpu.VMEM((8, 4, 2, ROWS, HD), BF),
            pltpu.VMEM((2, 4, 4, 4, ROWS, HD), BF),
            pltpu.VMEM((4, 4, HD, ROWS), BF),
            pltpu.VMEM((16, 2, 2, ROWS, HD), BF),
            pltpu.VMEM((2, 8, ROWS, ROWS), F32),
            pltpu.VMEM((16, HD, ROWS), F32),
            pltpu.VMEM((16, 8, ROWS), F32),
            pltpu.VMEM((16, 8, ROWS), F32),
            pltpu.VMEM((4, 4, ROWS, HD), BF),
            pltpu.VMEM((4, 4, ROWS, HD), BF),
            pltpu.VMEM((2, 4, 128, HD), BF),
            pltpu.VMEM((8, ROWS, 256), F32),
            pltpu.VMEM((4, ROWS, 512), BF),
            dma((7,)),
            *pair(6), *pair(2, 4), *pair(2, 4, 4), *pair(2, 4, 4),
            *pair(3), *pair(4), *pair(4, 4), *pair(4, 4),
            *pair(4, 6), *pair(3, 2, 2), *pair(2, 2), dma((4,)),
        ],
        compiler_params=pltpu.CompilerParams(
            collective_id=0, has_side_effects=True, vmem_limit_bytes=56 * 1024 * 1024
        ),
    )(tokens, w_query, w_key.T, w_value.T, w_out, qk_gain, jnp.asarray(cos_t), jnp.asarray(sin_t))
    return out[None]


def solution(mesh):
    in_specs = (
        P("dp", "sp", None),
        P("dp", "sp"),
        P("dp", "sp"),
        P("dp", "sp"),
        P("dp", "sp"),
        P(),
    )
    out_specs = P("dp", "sp", None)
    return jax.shard_map(
        on_device, mesh=mesh, in_specs=in_specs, out_specs=out_specs, check_vma=False
    )
```

time: 88.3 us -> 85.8 us (0.972)
  Pallas kernels: 85.7 us -> 83.3 us
    pallas_call x1, Pallas kernels: 85.7 us -> 83.3 us  [on_device(): pl.pallas_call(kernel, out_shape=jax.ShapeDtypeStruct((ROWS, 2048), BF),...]
where the time goes in v3:
time: 85.8 us; the launch traced here: 85.6 us
  Pallas kernels  83.3 us (97%)
  local copies, waits for them, and re-layouts  2.3 us (3%)
    pallas_call x1, Pallas kernels, on_device(): pl.pallas_call(kernel, out_shape=jax.ShapeDtypeStruct((ROWS, 2048), BF),...  83.3 us
    unnamed x1, local copies, waits for them, and re-layouts  2.3 us

profile of v3, /device:TPU:1, one launch (start us, length us, event | category | flops | bytes accessed | tf_op | source)
XLA Modules:
  0.0 85.6 jit_solution(3344950741073156314)
XLA Ops:
  0.0 83.3 %shard_map.82 = bf16[256,2048]{1,0:T(8,128)(2,1)} custom-call(bf16[1,256,2048]{2,1,0:T(8,128)(2,1)} %tok_hbm.1, bf16[256,128]{1,0:T(8,128)(2,1)} %wq_hbm.1, bf16[64,256]{1,0:T(8,128)(2,1)} %bitcast.4, bf16[64,256]{1,0:T(8,128)(2,1)} %bitcast.5, bf16[256,128]{1,0:T(8,128)(2,1)} %wo_hbm.1, f32[2,128]{1,0:T(2,128)} %gain_ref.1, ...), custom_call_target="tpu_custom_call" | custom-call | tf_op jit(solution)/shard_map/pallas_call | solution.py:622
  83.3 2.3 %copy.10 = bf16[1,256,2048]{2,1,0:T(8,128)(2,1)} copy(bf16[1,256,2048]{2,1,0:T(8,128)(2,1)} %bitcast.3) | data formatting | bytes 2097152

commit v4 on v3

--- a/solution.py
+++ b/solution.py
@@ -50,8 +50,9 @@
 
 
 def kernel(
-    tok_hbm, wq_hbm, wk_hbm, wv_hbm, wo_hbm, gain_ref, cos_ref, sin_ref,
+    tok_hbm, wq_hbm, wk_hbm, wv_hbm, wo_hbm, gain_hbm, cos_hbm, sin_hbm,
     out_ref,
+    gain_ref, cos_ref, sin_ref,
     X, W, WO, QT, KVB, S, ACC, MX, LS, AO, ATT, RB, OF, OB,
     loc, tok_s, tok_r, w1_s, w1_r, w2_s, w2_r, wp_s, wp_r,
     o1_s, o1_r, o2_s, o2_r, o3_s, o3_r, op_s, op_r,
@@ -85,8 +86,11 @@
         (wk_hbm.at[:, hi], W.at[dp, y, 1, pl.ds(128, 64)]),
         (wv_hbm.at[:, lo], W.at[dp, y, 1, pl.ds(64, 64)]),
         (wv_hbm.at[:, hi], W.at[dp, y, 1, pl.ds(192, 64)]),
-        (wo_hbm, WO.at[c, x, y, z]),
+        (wo_hbm, WO.at[c, x, y * (1 - c) + z * c, z * (1 - c) + y * c]),
         (tok_hbm.at[0], X.at[0]),
+        (gain_hbm, gain_ref),
+        (cos_hbm, cos_ref),
+        (sin_hbm, sin_ref),
     ]
     local = [pltpu.make_async_copy(a, b, loc.at[i]) for i, (a, b) in enumerate(local)]
     for one in local:
@@ -150,11 +154,12 @@
         b = wslot(1 - c, r, d, p)
         return to(b, b, wp_s.at[p, r, d], wp_r.at[p, r, d], other=True)
 
-    oa, ob, oc = x, y, z
+    oa, ob, oc = x, y * (1 - c) + z * c, z * (1 - c) + y * c
 
     def o1(d):
         return to(
-            wo_hbm, WO.at[c, oa, ob, oc], o1_s.at[d - 1], o1_r.at[d - 1], dz=d
+            wo_hbm, WO.at[c, oa, ob, oc], o1_s.at[d - 1], o1_r.at[d - 1],
+            dz=d * (1 - c), dy=d * c,
         )
 
     def o1_in(d):
@@ -164,7 +169,7 @@
     two = lambda ref, i: ref.at[pl.ds(2 * i, 2)]
     o2 = Ring(
         to, lambda d: WO.at[c, oa, ring(ob, d)], two,
-        lambda d: dict(dy=d), lambda k: o2_s.at[k], lambda k: o2_r.at[k],
+        lambda d: dict(dy=d * (1 - c), dz=d * c), lambda k: o2_s.at[k], lambda k: o2_r.at[k],
     )
     o3 = [
         Ring(
@@ -179,7 +184,7 @@
         return to(b, b, op_s.at[r, d], op_r.at[r, d], other=True)
 
     def op_in(r, d):
-        b = WO.at[1 - c, ring(oa, d), ring(y, r)]
+        b = WO.at[1 - c, ring(oa, d), ring(y * c + z * (1 - c), r)]
         return to(b, b, op_s.at[r, d], op_r.at[r, d], other=True)
 
     def kvc(v, i, landing=False):
@@ -251,8 +256,11 @@
             for d in (0, 3, 1, 2):
                 wp_in(p, r, d).wait_recv()
 
-    for d in (2, 1, 3):
-        o1(d).start()
+    def o1_send():
+        for d in (2, 1, 3):
+            o1(d).start()
+
+    pl.when(c == 0)(o1_send)
     for i in range(4):
         tok(i).start()
     for i in range(4):
@@ -297,11 +305,12 @@
     w1_far(0)
     for r in order:
         w2_send(0, r)
-    pl.when(c == 1)(o2_send)
+    pl.when(c == 1)(o1_send)
     for r in order:
         w2_far(1, r)
     wp_wait(1)
-    local[6].wait()
+    for i in range(6, 10):
+        local[i].wait()
     lane = lax.broadcasted_iota(jnp.int32, (64, HD), 1)
     low64 = lane < 64
     even = lane % 2 == 0
@@ -484,12 +493,17 @@
     kv_and_send(0)
     for r in order:
         w2_near(0, r)
-    o3_send(0)
+    pl.when(c == 0)(lambda: o3_send(0))
     for i in range(2):
         tok(i).wait_recv()
         tok(i + 4).start()
+
+    @pl.when(c == 1)
+    def _():
+        o2_send()
+        o3_send(0)
     kv_and_send(1)
-    o2_pass_on()
+    pl.when(c == 0)(o2_pass_on)
     for r in order:
         w2_far(0, r)
     wp_wait(0)
@@ -507,17 +521,22 @@
     project_q(2)
     run_units(4, first_two, set_b)
     run_units(2, lambda u: (2, u), set_a + set_b)
-    o2_far()
+    pl.when(c == 0)(o2_far)
     kv_pass_on(1)
     kv_near(1)
     kv_far(0)
     o3_pass_on(0)
-    o3_pass_on(3)
+    pl.when(c == 0)(lambda: o3_pass_on(3))
     run_units(6, first_two, set_d)
     tok(4).wait_recv()
     tok(5).wait_recv()
     kv_and_send(3)
     project_q(3)
+    pl.when(c == 1)(o2_pass_on)
+
+    def on_core(core, event, *rs):
+        return lambda: pl.when(c == core)(lambda: event(*rs))
+
     run_units(2, lambda u: (3, u), set_a + set_b + set_d)
     kv_pass_on(2)
     kv_near(2)
@@ -526,9 +545,12 @@
     run_units(
         8, first_two, ((0, 3), (2, 1), (1, 2), (3, 2)),
         events=(
-            (0, lambda: o3_pass_on(1, 2)),
+            (0, on_core(0, o3_pass_on, 1, 2)),
+            (0, on_core(1, o2_far)),
             (2, lambda: kv_pass_on(3)),
-            (5, lambda: o3_far(0, 3)),
+            (5, lambda: o3_far(0)),
+            (5, on_core(0, o3_far, 3)),
+            (6, on_core(1, o3_pass_on, 3, 1)),
         ),
     )
     kv_far(2)
@@ -544,9 +566,15 @@
     run_units(4, lambda u: (3 - u, 0), last, finish=finish)
     run_units(
         4, lambda u: (3 - u, 1), last, finish=finish,
-        events=((0, lambda: o3_far(1, 2)), (1, lambda: relay(0))),
+        events=(
+            (0, on_core(0, o3_far, 1, 2)),
+            (0, on_core(1, o3_far, 3, 1)),
+            (1, on_core(1, o3_pass_on, 2)),
+            (1, lambda: relay(0)),
+        ),
     )
     relay(1)
+    on_core(1, o3_far, 2)()
     def out_terms(n, who):
         zc, yc = n // 2, (n % 2) * 2
         total = None
@@ -555,7 +583,10 @@
             for i in range(2):
                 src = AO.at[0] if r == 0 else ATT.at[zs]
                 lhs = jnp.concatenate([src[2 * i], src[2 * i + 1]], axis=1)
-                cols = [WO[i, zs, yc, zc], WO[i, zs, yc + 1, zc]]
+                if i == 0:
+                    cols = [WO[0, zs, yc, zc], WO[0, zs, yc + 1, zc]]
+                else:
+                    cols = [WO[1, zs, zc, yc], WO[1, zs, zc, yc + 1]]
                 d = jnp.dot(lhs, jnp.concatenate(cols, axis=1), preferred_element_type=F32)
                 total = d if total is None else total + d
         return total
@@ -622,9 +653,12 @@
     out = pl.pallas_call(
         kernel,
         out_shape=jax.ShapeDtypeStruct((ROWS, 2048), BF),
-        in_specs=[any_, any_, any_, any_, any_, vm, vm, vm],
+        in_specs=[any_] * 8,
         out_specs=any_,
         scratch_shapes=[
+            pltpu.VMEM((2, HD), F32),
+            pltpu.VMEM((GRID_W, HD), F32),
+            pltpu.VMEM((GRID_W, HD), F32),
             pltpu.VMEM((4, ROWS, 2048), BF),
             pltpu.VMEM((8, 4, 2, ROWS, HD), BF),
             pltpu.VMEM((2, 4, 4, 4, ROWS, HD), BF),
@@ -639,7 +673,7 @@
             pltpu.VMEM((2, 4, 128, HD), BF),
             pltpu.VMEM((8, ROWS, 256), F32),
             pltpu.VMEM((4, ROWS, 512), BF),
-            dma((7,)),
+            dma((10,)),
             *pair(6), *pair(2, 4), *pair(2, 4, 4), *pair(2, 4, 4),
             *pair(3), *pair(4), *pair(4, 4), *pair(4, 4),
             *pair(4, 6), *pair(3, 2, 2), *pair(2, 2), dma((4,)),

time: 85.8 us -> 81.8 us (0.953)
  Pallas kernels: 83.3 us -> 79.3 us
    pallas_call x1, Pallas kernels: 83.3 us -> 79.3 us  [on_device(): pl.pallas_call(kernel, out_shape=jax.ShapeDtypeStruct((ROWS, 2048), BF),...]
where the time goes in v4:
time: 81.8 us; the launch traced here: 81.6 us
  Pallas kernels  79.3 us (97%)
  local copies, waits for them, and re-layouts  2.3 us (3%)
    pallas_call x1, Pallas kernels, on_device(): pl.pallas_call(kernel, out_shape=jax.ShapeDtypeStruct((ROWS, 2048), BF),...  79.3 us
    unnamed x1, local copies, waits for them, and re-layouts  2.3 us

profile of v4, /device:TPU:1, one launch (start us, length us, event | category | flops | bytes accessed | tf_op | source)
XLA Modules:
  0.0 81.6 jit_solution(7375611534909631391)
XLA Ops:
  0.0 79.3 %shard_map.82 = bf16[256,2048]{1,0:T(8,128)(2,1)} custom-call(bf16[1,256,2048]{2,1,0:T(8,128)(2,1)} %tok_hbm.1, bf16[256,128]{1,0:T(8,128)(2,1)} %wq_hbm.1, bf16[64,256]{1,0:T(8,128)(2,1)} %bitcast.4, bf16[64,256]{1,0:T(8,128)(2,1)} %bitcast.5, bf16[256,128]{1,0:T(8,128)(2,1)} %wo_hbm.1, f32[2,128]{1,0:T(2,128)} %gain_hbm.1, ...), custom_call_target="tpu_custom_call" | custom-call | tf_op jit(solution)/shard_map/pallas_call | solution.py:653
  79.3 2.3 %copy.10 = bf16[1,256,2048]{2,1,0:T(8,128)(2,1)} copy(bf16[1,256,2048]{2,1,0:T(8,128)(2,1)} %bitcast.3) | data formatting | bytes 2097152

commit v5 on v4

--- a/solution.py
+++ b/solution.py
@@ -531,8 +531,8 @@
     tok(4).wait_recv()
     tok(5).wait_recv()
     kv_and_send(3)
+    pl.when(c == 1)(o2_pass_on)
     project_q(3)
-    pl.when(c == 1)(o2_pass_on)
 
     def on_core(core, event, *rs):
         return lambda: pl.when(c == core)(lambda: event(*rs))
@@ -568,9 +568,9 @@
         4, lambda u: (3 - u, 1), last, finish=finish,
         events=(
             (0, on_core(0, o3_far, 1, 2)),
-            (0, on_core(1, o3_far, 3, 1)),
+            (1, lambda: relay(0)),
             (1, on_core(1, o3_pass_on, 2)),
-            (1, lambda: relay(0)),
+            (2, on_core(1, o3_far, 3, 1)),
         ),
     )
     relay(1)

time: 81.8 us -> 81.2 us (level)
  Pallas kernels: 79.3 us -> 78.4 us
    pallas_call x1, Pallas kernels: 79.3 us -> 78.4 us  [on_device(): pl.pallas_call(kernel, out_shape=jax.ShapeDtypeStruct((ROWS, 2048), BF),...]
where the time goes in v5:
time: 81.2 us; the launch traced here: 80.7 us
  Pallas kernels  78.4 us (97%)
  local copies, waits for them, and re-layouts  2.3 us (3%)
    pallas_call x1, Pallas kernels, on_device(): pl.pallas_call(kernel, out_shape=jax.ShapeDtypeStruct((ROWS, 2048), BF),...  78.4 us
    unnamed x1, local copies, waits for them, and re-layouts  2.3 us

profile of v5, /device:TPU:1, one launch (start us, length us, event | category | flops | bytes accessed | tf_op | source)
XLA Modules:
  0.0 80.7 jit_solution(937581040342086122)
XLA Ops:
  0.0 78.4 %shard_map.82 = bf16[256,2048]{1,0:T(8,128)(2,1)} custom-call(bf16[1,256,2048]{2,1,0:T(8,128)(2,1)} %tok_hbm.1, bf16[256,128]{1,0:T(8,128)(2,1)} %wq_hbm.1, bf16[64,256]{1,0:T(8,128)(2,1)} %bitcast.4, bf16[64,256]{1,0:T(8,128)(2,1)} %bitcast.5, bf16[256,128]{1,0:T(8,128)(2,1)} %wo_hbm.1, f32[2,128]{1,0:T(2,128)} %gain_hbm.1, ...), custom_call_target="tpu_custom_call" | custom-call | tf_op jit(solution)/shard_map/pallas_call | solution.py:653
  78.4 2.3 %copy.10 = bf16[1,256,2048]{2,1,0:T(8,128)(2,1)} copy(bf16[1,256,2048]{2,1,0:T(8,128)(2,1)} %bitcast.3) | data formatting | bytes 2097152

commit v6 on v5

--- a/solution.py
+++ b/solution.py
@@ -550,7 +550,6 @@
             (2, lambda: kv_pass_on(3)),
             (5, lambda: o3_far(0)),
             (5, on_core(0, o3_far, 3)),
-            (6, on_core(1, o3_pass_on, 3, 1)),
         ),
     )
     kv_far(2)
@@ -563,7 +562,10 @@
             relay_out(g, half).start()
 
     last = ((2, 2), (1, 3), (3, 3), (2, 3))
-    run_units(4, lambda u: (3 - u, 0), last, finish=finish)
+    run_units(
+        4, lambda u: (3 - u, 0), last, finish=finish,
+        events=((0, on_core(1, o3_pass_on, 3, 1)),),
+    )
     run_units(
         4, lambda u: (3 - u, 1), last, finish=finish,
         events=(

time: 81.2 us -> 81.2 us (level)
  no operation moved by 1% of the time
where the time goes in v6:
time: 81.2 us; the launch traced here: 80.7 us
  Pallas kernels  78.4 us (97%)
  local copies, waits for them, and re-layouts  2.3 us (3%)
    pallas_call x1, Pallas kernels, on_device(): pl.pallas_call(kernel, out_shape=jax.ShapeDtypeStruct((ROWS, 2048), BF),...  78.4 us
    unnamed x1, local copies, waits for them, and re-layouts  2.3 us

profile of v6, /device:TPU:1, one launch (start us, length us, event | category | flops | bytes accessed | tf_op | source)
XLA Modules:
  0.0 80.7 jit_solution(9513033133175459804)
XLA Ops:
  0.0 78.4 %shard_map.82 = bf16[256,2048]{1,0:T(8,128)(2,1)} custom-call(bf16[1,256,2048]{2,1,0:T(8,128)(2,1)} %tok_hbm.1, bf16[256,128]{1,0:T(8,128)(2,1)} %wq_hbm.1, bf16[64,256]{1,0:T(8,128)(2,1)} %bitcast.4, bf16[64,256]{1,0:T(8,128)(2,1)} %bitcast.5, bf16[256,128]{1,0:T(8,128)(2,1)} %wo_hbm.1, f32[2,128]{1,0:T(2,128)} %gain_hbm.1, ...), custom_call_target="tpu_custom_call" | custom-call | tf_op jit(solution)/shard_map/pallas_call | solution.py:655
  78.4 2.3 %copy.10 = bf16[1,256,2048]{2,1,0:T(8,128)(2,1)} copy(bf16[1,256,2048]{2,1,0:T(8,128)(2,1)} %bitcast.3) | data formatting | bytes 2097152
